TPU v7x, 32 devices: a whole 2x2x4 slice. The times are simulated.
32 devices in a mesh: sp: 4 (over y, x), tp: 8 (over z, core).
Axes of the slice: x: 2, y: 2, z: 4, core: 2. Of those that a mesh axis runs over, the one named last changes fastest.
Arguments:
- latent: bfloat16 [4096, 2048], P(('sp', 'tp')), may hold values from -1.5 to 1.5
- context: bfloat16 [128, 2048], P('sp'), may hold values from -6 to 6
- cond: bfloat16 [2048], replicated, may hold values from -6 to 6
- cond_context: bfloat16 [2048], replicated, may hold values from -6 to 6
- mod_weight: bfloat16 [3, 2048, 2048], P(None, 'sp', 'tp'), may hold values from -0.125 to 0.125
- norm_gain: bfloat16 [2048], replicated, may hold values from 0.099609375 to 1.8984375
- down_q: bfloat16 [2048, 768], P('tp'), may hold values from -0.125 to 0.125
- down_kv: bfloat16 [2048, 512], P('tp'), may hold values from -0.125 to 0.125
- rope_weight: bfloat16 [2048, 32], replicated, may hold values from -0.125 to 0.125
- qlat_gain: bfloat16 [768], replicated, may hold values from 0.099609375 to 1.8984375
- kvlat_gain: bfloat16 [512], replicated, may hold values from 0.099609375 to 1.8984375
- up_query: bfloat16 [768, 1536], P(None, 'tp'), may hold values from -0.21875 to 0.21875
- up_key: bfloat16 [512, 1024], P(None, 'tp'), may hold values from -0.25 to 0.25
- up_value: bfloat16 [512, 1024], P(None, 'tp'), may hold values from -0.25 to 0.25
- query_gain: float32 [96], replicated, may hold values from 0.5 to 8
- key_gain: float32 [96], replicated, may hold values from 0.5 to 8
- context_bias: float32 [16], P('tp'), may hold values from -2.2 to -0.7
- out_weight: bfloat16 [1024, 2048], P('tp'), may hold values from -24 to 24
Outputs:
- mixed: bfloat16 [4096, 2048], P(('sp', 'tp'))
All inputs are finite; a program needn't handle non-finite values.
Results may differ from a plain program's by a relative error of at most 0.028.
The roundings to bfloat16 on the way count: a program that leaves them out, or rounds other values in their place, can miss the bound.
Values may be sent and summed in bfloat16 or wider, within the bound.
A program may use at most 64 MiB of HBM per device.

v0:
```python
import math

import jax
import jax.numpy as jnp
from jax import lax
from jax.sharding import PartitionSpec as P

NOPE = 64
ROPE = 32
VDIM = 64
GRID_W = 64
TOK_DEV = 1024
CTX_DEV = 32


epsilon = 1e-06
theta = 10000.0


def rms_scale(tensor, gain):
    return (
        tensor
        * lax.rsqrt(jnp.mean(tensor * tensor, axis=-1, keepdims=True) + epsilon)
        * gain.astype(jnp.float32)
    )


def axial_tables(positions):
    pair_count = ROPE // 4
    frequency = jnp.power(theta, -jnp.arange(pair_count, dtype=jnp.float32) / pair_count)
    row_angle = (positions // GRID_W).astype(jnp.float32)[:, None] * frequency
    col_angle = (positions % GRID_W).astype(jnp.float32)[:, None] * frequency
    return (jnp.cos(row_angle), jnp.sin(row_angle), jnp.cos(col_angle), jnp.sin(col_angle))


def rotate_half(tensor, cosine, sine_table):
    first, second = jnp.split(tensor, 2, axis=-1)
    cosine = cosine[:, None, :]
    sine_table = sine_table[:, None, :]
    return jnp.concatenate(
        [first * cosine - second * sine_table, second * cosine + first * sine_table], axis=-1
    )


def axial_rotate(tensor, tables):
    half_width = tensor.shape[-1] // 2
    return jnp.concatenate(
        [
            rotate_half(tensor[..., :half_width], tables[0], tables[1]),
            rotate_half(tensor[..., half_width:], tables[2], tables[3]),
        ],
        axis=-1,
    )


def modulate(row_block, gain, shifts, scales):
    normal = rms_scale(row_block.astype(jnp.float32), gain)
    return (normal * (1.0 + scales) + shifts).astype(jnp.bfloat16)


def make_queries(query_latent, up_query, query_gain, tables):
    amount = query_latent.shape[0]
    projected = jnp.dot(query_latent, up_query, preferred_element_type=jnp.float32).reshape(
        amount, -1, NOPE + ROPE
    )
    normal = rms_scale(projected, query_gain)
    return jnp.concatenate(
        [normal[..., :NOPE], axial_rotate(normal[..., NOPE:], tables)], axis=-1
    ).astype(jnp.bfloat16)


def make_keys(kv_latent, rope_rows, up_key, up_value, key_gain, tables):
    amount = kv_latent.shape[0]
    unrotated = jnp.dot(kv_latent, up_key, preferred_element_type=jnp.float32).reshape(
        amount, -1, NOPE
    )
    head_count = unrotated.shape[1]
    shared = jnp.broadcast_to(rope_rows.astype(jnp.float32)[:, None, :], (amount, head_count, ROPE))
    normal = rms_scale(jnp.concatenate([unrotated, shared], axis=-1), key_gain)
    if tables is not None:
        normal = jnp.concatenate(
            [normal[..., :NOPE], axial_rotate(normal[..., NOPE:], tables)], axis=-1
        )
    values = jnp.dot(kv_latent, up_value, preferred_element_type=jnp.float32).reshape(
        amount, head_count, VDIM
    )
    return (normal.astype(jnp.bfloat16), values.astype(jnp.bfloat16))


def absorb_block(state_in, queries, key_block, value_block, shift_heads):
    run_max, run_sum, run_acc = state_in
    scores = jnp.einsum("qhd,khd->qhk", queries, key_block, preferred_element_type=jnp.float32) * (
        NOPE + ROPE
    ) ** (-0.5)
    scores = scores + shift_heads[None, :, None]
    new_max = jnp.maximum(run_max, jnp.max(scores, axis=-1))
    factor = jnp.exp(run_max - new_max)
    weights = jnp.exp(scores - new_max[..., None])
    run_sum = run_sum * factor + jnp.sum(weights, axis=-1)
    run_acc = run_acc * factor[..., None] + jnp.einsum(
        "qhk,khd->qhd",
        weights.astype(jnp.bfloat16),
        value_block,
        preferred_element_type=jnp.float32,
    )
    return (new_max, run_sum, run_acc)


def shards(
    latent,
    context,
    cond,
    cond_context,
    mod_weight,
    norm_gain,
    down_q,
    down_kv,
    rope_weight,
    qlat_gain,
    kvlat_gain,
    up_query,
    up_key,
    up_value,
    query_gain,
    key_gain,
    context_bias,
    out_weight,
):
    seq_index = lax.axis_index("sp")
    tp_count = lax.axis_size("tp")
    own_rows = latent.shape[0]
    block_tokens = own_rows * tp_count
    row_span = mod_weight.shape[1]
    activated = jax.nn.silu(jnp.stack([cond, cond_context]).astype(jnp.float32)).astype(
        jnp.bfloat16
    )
    own_part = lax.dynamic_slice_in_dim(activated, seq_index * row_span, row_span, 1)
    partial_value = jnp.concatenate(
        [
            jnp.einsum("d,rde->re", own_part[0], mod_weight, preferred_element_type=jnp.float32),
            jnp.einsum(
                "d,rde->re", own_part[1], mod_weight[:2], preferred_element_type=jnp.float32
            ),
        ],
        axis=0,
    )
    summed = lax.psum(partial_value, "sp")
    modulations = lax.all_gather(summed, "tp", axis=1, tiled=True)
    normed = modulate(latent, norm_gain, modulations[0], modulations[1])
    context_normed = modulate(context, norm_gain, modulations[3], modulations[4])
    stacked = jnp.concatenate([normed, context_normed], axis=0)
    pieces = (
        lax.all_gather(down_q, "tp", axis=0, tiled=True),
        lax.all_gather(down_kv, "tp", axis=0, tiled=True),
    )
    columns = stacked
    query_down = jnp.dot(columns[:own_rows], pieces[0], preferred_element_type=jnp.float32)
    kv_down = jnp.dot(columns, pieces[1], preferred_element_type=jnp.float32)
    query_latent = rms_scale(query_down, qlat_gain).astype(jnp.bfloat16)
    kv_latent = rms_scale(kv_down, kvlat_gain).astype(jnp.bfloat16)
    rope_rows = jnp.dot(stacked, rope_weight, preferred_element_type=jnp.float32).astype(
        jnp.bfloat16
    )
    all_query, all_kv, all_rope = (
        lax.all_gather(query_latent, "tp", axis=0, tiled=True),
        lax.all_gather(kv_latent[:own_rows], "tp", axis=0, tiled=True),
        lax.all_gather(rope_rows[:own_rows], "tp", axis=0, tiled=True),
    )
    own_context_keys, own_context_values = make_keys(
        kv_latent[own_rows:], rope_rows[own_rows:], up_key, up_value, key_gain, None
    )
    context_keys, context_values = (
        lax.all_gather(own_context_keys, "sp", axis=0, tiled=True),
        lax.all_gather(own_context_values, "sp", axis=0, tiled=True),
    )
    positions = seq_index * block_tokens + jnp.arange(block_tokens, dtype=jnp.int32)
    tables = axial_tables(positions)
    queries = make_queries(all_query, up_query, query_gain, tables)
    keys, values = make_keys(all_kv, all_rope, up_key, up_value, key_gain, tables)
    head_count = queries.shape[1]
    shift_heads = context_bias + math.log(TOK_DEV / CTX_DEV)
    start_state = (
        jnp.full((block_tokens, head_count), -jnp.inf, jnp.float32),
        jnp.zeros((block_tokens, head_count), jnp.float32),
        jnp.zeros((block_tokens, head_count, VDIM), jnp.float32),
    )
    state_now = absorb_block(start_state, queries, context_keys, context_values, shift_heads)
    no_shift = jnp.zeros((head_count,), jnp.float32)
    pieces = (
        lax.all_gather(keys, "sp", axis=0, tiled=True),
        lax.all_gather(values, "sp", axis=0, tiled=True),
    )
    amount = pieces[0].shape[0]
    span_rows = math.gcd(amount, 1024)
    key_blocks = pieces[0].reshape(amount // span_rows, span_rows, head_count, pieces[0].shape[2])
    value_blocks = pieces[1].reshape(amount // span_rows, span_rows, head_count, pieces[1].shape[2])

    def scan_step(state_mid, blocks):
        return (absorb_block(state_mid, queries, blocks[0], blocks[1], no_shift), None)

    state_out, unused = lax.scan(scan_step, state_now, (key_blocks, value_blocks))
    run_max, run_sum, run_acc = state_out
    attended = (
        (run_acc / run_sum[..., None]).astype(jnp.bfloat16).reshape(block_tokens, head_count * VDIM)
    )
    token_rows = lax.all_to_all(attended, "tp", split_axis=0, concat_axis=1, tiled=True)
    columns = token_rows
    projected = jnp.dot(
        columns,
        lax.all_gather(out_weight, "tp", axis=0, tiled=True),
        preferred_element_type=jnp.float32,
    )
    return (latent.astype(jnp.float32) + modulations[2] * projected).astype(jnp.bfloat16)


def solution(mesh):
    in_specs = (
        P(("sp", "tp"), None),
        P("sp", None),
        P(),
        P(),
        P(None, "sp", "tp"),
        P(),
        P("tp", None),
        P("tp", None),
        P(),
        P(),
        P(),
        P(None, "tp"),
        P(None, "tp"),
        P(None, "tp"),
        P(),
        P(),
        P("tp"),
        P("tp", None),
    )
    out_specs = P(("sp", "tp"), None)
    return jax.shard_map(shards, mesh=mesh, in_specs=in_specs, out_specs=out_specs, check_vma=False)
```

profile of v0, /device:TPU:0, one launch (start us, length us, event | category | flops | bytes accessed | tf_op | source)
XLA Modules:
  0.0 254.6 jit_solution(11585700958939711861)
XLA Ops:
  13.5 11.5 %psum.7 = f32[5,256]{1,0:T(8,128)S(1)} all-reduce(f32[5,256]{1,0:T(8,128)S(1)} %pad_maximum_fusion.5), channel_id=1, replica_groups=mesh['sp'=4,'tp'=8] {'sp'}, use_global_device_ids=true, to_apply=%region_0.1 | all-reduce | flops 1280 | bytes 10240 | tf_op jit(solution)/shard_map/psum | solution.py:147
  25.0 14.7 %all_gather.33 = f32[5,2048]{1,0:T(8,128)S(1)} all-gather(f32[5,256]{1,0:T(8,128)S(1)} %psum.7), channel_id=1, replica_groups=mesh['sp'=4,'tp'=8] {'tp'}, dimensions={1}, use_global_device_ids=true | all-gather | bytes 46080 | tf_op jit(solution)/shard_map/all_gather | solution.py:148
  44.4 2.2 multiply_reduce_fusion.3
  47.6 33.1 %all-gather.10.cloned.1.call-done = bf16[2048,768]{1,0:T(8,128)(2,1)} async-done(((bf16[256,768]{1,0:T(8,128)(2,1)}), bf16[2048,768]{1,0:T(8,128)(2,1)}) %all-gather.10.cloned.1.call-update) | async-done | bytes 3145744 | tf_op jit(solution)/shard_map/all_gather | solution.py:153
  80.7 2.6 %multiply_reduce_fusion.2 = (f32[128]{0:T(128)S(1)}, f32[128,768]{1,0:T(8,128)S(1)}) fusion(bf16[128,2048]{1,0:T(8,128)(2,1)S(1)} %fusion.28, bf16[2048,768]{1,0:T(8,128)(2,1)} %all-gather.10.cloned.1.call-done), kind=kOutput, calls=%fused_computation.55 | convolution fusion | flops 402849664 | bytes 4063744 | tf_op jit(solution)/shard_map/dot_general | solution.py:157
  84.4 13.1 %all_gather.40 = bf16[1024,32]{0,1:T(8,128)(2,1)S(1)} all-gather(bf16[128,32]{0,1:T(8,128)(2,1)S(1)} %slice.87), channel_id=1, replica_groups=mesh['sp'=4,'tp'=8] {'tp'}, dimensions={0}, use_global_device_ids=true | all-gather | bytes 73728 | tf_op jit(solution)/shard_map/all_gather | solution.py:167
  97.9 5.5 %all-gather.14.cloned.1.call-done = bf16[1024,512]{1,0:T(8,128)(2,1)} async-done(((bf16[128,512]{1,0:T(8,128)(2,1)}), bf16[1024,512]{1,0:T(8,128)(2,1)}) %all-gather.14.cloned.1.call-update) | async-done | bytes 1048592 | tf_op jit(solution)/shard_map/all_gather | solution.py:166
  103.4 1.8 fusion.69
  106.8 23.0 %all-gather.12.cloned.1.call-done = bf16[1024,768]{1,0:T(8,128)(2,1)} async-done(((bf16[128,768]{1,0:T(8,128)(2,1)}), bf16[1024,768]{1,0:T(8,128)(2,1)}) %all-gather.12.cloned.1.call-update) | async-done | bytes 1572880 | tf_op jit(solution)/shard_map/all_gather | solution.py:165
  129.8 2.1 fusion.68
  134.6 8.7 %all_gather.35 = bf16[128,2,96]{2,0,1:T(8,128)(2,1)S(1)} all-gather(bf16[32,2,96]{2,0,1:T(8,128)(2,1)S(1)} %multiply_convert_fusion.2), channel_id=1, replica_groups=mesh['sp'=4,'tp'=8] {'sp'}, dimensions={0}, use_global_device_ids=true | all-gather | bytes 61440 | tf_op jit(solution)/shard_map/all_gather | solution.py:173
  143.3 8.2 %all_gather.38 = bf16[128,2,64]{2,0,1:T(8,128)(2,1)S(1)} all-gather(bf16[32,2,64]{2,0,1:T(8,128)(2,1)S(1)} %copy.43), channel_id=1, replica_groups=mesh['sp'=4,'tp'=8] {'sp'}, dimensions={0}, use_global_device_ids=true | all-gather | bytes 40960 | tf_op jit(solution)/shard_map/all_gather | solution.py:174
  151.6 5.9 %all-gather.18.cloned.1.call-done = bf16[4096,2,64]{0,2,1:T(8,128)(2,1)} async-done(((bf16[1024,2,64]{0,2,1:T(8,128)(2,1)}), bf16[4096,2,64]{0,2,1:T(8,128)(2,1)}) %all-gather.18.cloned.1.call-update) | async-done | bytes 1048592 | tf_op jit(solution)/shard_map/all_gather | solution.py:191
  157.4 2.3 copy.60
  160.5 29.4 %all-gather.16.cloned.1.call-done = bf16[4096,2,96]{0,2,1:T(8,128)(2,1)} async-done(((bf16[1024,2,96]{0,2,1:T(8,128)(2,1)}), bf16[4096,2,96]{0,2,1:T(8,128)(2,1)}) %all-gather.16.cloned.1.call-update) | async-done | bytes 1572880 | tf_op jit(solution)/shard_map/all_gather | solution.py:190
  189.9 1.6 copy.59
  191.5 21.5 %while.14 = (s32[]{:T(128)}, f32[1024,2]{0,1:T(2,128)S(1)}, f32[1024,2]{0,1:T(2,128)S(1)}, f32[1024,2,64]{0,2,1:T(8,128)S(1)}, bf16[4,1024,2,96]{1,3,2,0:T(8,128...) while((s32[]{:T(128)}, f32[1024,2]{0,1:T(2,128)S(1)}, ...), condition=%wide.region_13.14_spmd, body=%wide.region_10.13_spmd.sunk | while | flops 688132096 | bytes 27394648 | solution.py:201
  194.3 2.6 %fusion.98 = f32[1024,2,64]{0,2,1:T(8,128)S(1)} fusion(f32[2,1024,1024]{2,1,0:T(8,128)S(1)} %get-tuple-element.168, f32[1024,2]{0,1:T(2,128)S(1)} %max.4, f32[1024,2,64]{0,2,1:T(8,128)S(1)} %get-tuple-element.182, bf16[4,1024,2,64]{1,3,2,0:T(8,128)(2,1)} %get-tuple-element.193, s32[]{:T(128)} %get-tuple-element.179, f32[1024,2]{0,1:T(2,128)S(1)} %get-tuple-element.170), kind=kOutput, calls=%fused_computation.7.clone.1 | convolution fusion | flops 274989056 | bytes 9716224 | tf_op jit(solution)/shard_map/while/body/eval_jaxpr/qhk,khd->qhd/dot_general | solution.py:100
  199.6 2.6 %fusion.98 = f32[1024,2,64]{0,2,1:T(8,128)S(1)} fusion(f32[2,1024,1024]{2,1,0:T(8,128)S(1)} %get-tuple-element.168, f32[1024,2]{0,1:T(2,128)S(1)} %max.4, f32[1024,2,64]{0,2,1:T(8,128)S(1)} %get-tuple-element.182, bf16[4,1024,2,64]{1,3,2,0:T(8,128)(2,1)} %get-tuple-element.193, s32[]{:T(128)} %get-tuple-element.179, f32[1024,2]{0,1:T(2,128)S(1)} %get-tuple-element.170), kind=kOutput, calls=%fused_computation.7.clone.1 | convolution fusion | flops 274989056 | bytes 9716224 | tf_op jit(solution)/shard_map/while/body/eval_jaxpr/qhk,khd->qhd/dot_general | solution.py:100
  205.0 2.6 %fusion.98 = f32[1024,2,64]{0,2,1:T(8,128)S(1)} fusion(f32[2,1024,1024]{2,1,0:T(8,128)S(1)} %get-tuple-element.168, f32[1024,2]{0,1:T(2,128)S(1)} %max.4, f32[1024,2,64]{0,2,1:T(8,128)S(1)} %get-tuple-element.182, bf16[4,1024,2,64]{1,3,2,0:T(8,128)(2,1)} %get-tuple-element.193, s32[]{:T(128)} %get-tuple-element.179, f32[1024,2]{0,1:T(2,128)S(1)} %get-tuple-element.170), kind=kOutput, calls=%fused_computation.7.clone.1 | convolution fusion | flops 274989056 | bytes 9716224 | tf_op jit(solution)/shard_map/while/body/eval_jaxpr/qhk,khd->qhd/dot_general | solution.py:100
  210.4 2.6 %fusion.98 = f32[1024,2,64]{0,2,1:T(8,128)S(1)} fusion(f32[2,1024,1024]{2,1,0:T(8,128)S(1)} %get-tuple-element.168, f32[1024,2]{0,1:T(2,128)S(1)} %max.4, f32[1024,2,64]{0,2,1:T(8,128)S(1)} %get-tuple-element.182, bf16[4,1024,2,64]{1,3,2,0:T(8,128)(2,1)} %get-tuple-element.193, s32[]{:T(128)} %get-tuple-element.179, f32[1024,2]{0,1:T(2,128)S(1)} %get-tuple-element.170), kind=kOutput, calls=%fused_computation.7.clone.1 | convolution fusion | flops 274989056 | bytes 9716224 | tf_op jit(solution)/shard_map/while/body/eval_jaxpr/qhk,khd->qhd/dot_general | solution.py:100
  213.9 4.6 %all-to-all-start = ((bf16[8,128,128]{1,2,0:T(8,128)(2,1)}), bf16[8,128,128]{1,2,0:T(8,128)(2,1)S(1)}, u32[]{:S(2)}, u32[]{:S(2)}) async-start(bf16[8,128,128]{1,2,0:T(8,128)(2,1)} %copy.47), calls=%async_computation | async-start | bytes 524288 | tf_op jit(solution)/shard_map/all_to_all | solution.py:206
  218.5 25.6 %all-gather.20.cloned.1.call-done = bf16[1024,2048]{1,0:T(8,128)(2,1)} async-done(((bf16[128,2048]{1,0:T(8,128)(2,1)}), bf16[1024,2048]{1,0:T(8,128)(2,1)}) %all-gather.20.cloned.1.call-update) | async-done | bytes 4194320 | tf_op jit(solution)/shard_map/all_gather | solution.py:210
  244.1 3.7 %fusion.20 = bf16[128,2048]{1,0:T(8,128)(2,1)} fusion(bf16[128,1024]{0,1:T(8,128)(2,1)S(1)} %bitcast.112, bf16[1024,2048]{1,0:T(8,128)(2,1)} %all-gather.20.cloned.1.call-done, bf16[128,2048]{1,0:T(8,128)(2,1)S(1)} %copy-done.1, f32[2048]{0:T(1024)S(1)} %bitcast.113), kind=kOutput, calls=%fused_computation.20 | convolution fusion | flops 537919488 | bytes 5513216 | tf_op jit(solution)/shard_map/dot_general | solution.py:208
  (121 shorter events, 30.7 us)
Async XLA Ops:
  6.5 123.3 %copy-start = (bf16[768,192]{0,1:T(8,128)(2,1)S(1)}, bf16[768,192]{0,1:T(8,128)(2,1)}, u32[]{:S(2)}) copy-start(bf16[768,192]{0,1:T(8,128)(2,1)} %param.31) | copy-start | bytes 884740
  6.5 37.9 %all-gather.8.cloned.1.call-start = ((), (), s32[]{:S(2)}) async-start(), calls=%async_computation.1 | async-start | bytes 2359296 | tf_op jit(solution)/shard_map/all_gather | solution.py:154
  7.3 40.3 %copy-start.7 = (bf16[768]{0:T(1024)(128)(2,1)S(1)}, bf16[768]{0:T(1024)(128)(2,1)}, u32[]{:S(2)}) copy-start(bf16[768]{0:T(1024)(128)(2,1)} %param.29) | copy-start | bytes 4612
  7.3 73.4 %all-gather.10.cloned.1.call-start = ((), (), s32[]{:S(2)}) async-start(), calls=%async_computation.2 | async-start | bytes 3538944 | tf_op jit(solution)/shard_map/all_gather | solution.py:153
  8.0 95.4 %all-gather.14.cloned.1.call-start = ((), (), s32[]{:S(2)}) async-start(), calls=%async_computation.4 | async-start | bytes 1179648 | tf_op jit(solution)/shard_map/all_gather | solution.py:166
  44.4 39.7 %copy-start.9 = (bf16[2048,32]{0,1:T(8,128)(2,1)S(1)}, bf16[2048,32]{0,1:T(8,128)(2,1)}, u32[]{:S(2)}) copy-start(bf16[2048,32]{0,1:T(8,128)(2,1)} %param.28) | copy-start | bytes 393220
  46.7 56.7 %copy-start.4 = (bf16[512,128]{1,0:T(8,128)(2,1)S(1)}, bf16[512,128]{1,0:T(8,128)(2,1)}, u32[]{:S(2)}) copy-start(bf16[512,128]{1,0:T(8,128)(2,1)} %param.32) | copy-start | bytes 393220
  47.5 82.3 %all-gather.12.cloned.1.call-start = ((), (), s32[]{:S(2)}) async-start(), calls=%async_computation.3 | async-start | bytes 1769472 | tf_op jit(solution)/shard_map/all_gather | solution.py:165
  47.5 57.8 %copy-start.6 = (f32[96]{0:T(128)S(1)}, f32[96]{0:T(128)}, u32[]{:S(2)}) copy-start(f32[96]{0:T(128)} %param.35) | copy-start | bytes 1156
  83.2 22.3 %copy-start.5 = (bf16[512,128]{1,0:T(8,128)(2,1)S(1)}, bf16[512,128]{1,0:T(8,128)(2,1)}, u32[]{:S(2)}) copy-start(bf16[512,128]{1,0:T(8,128)(2,1)} %param.33) | copy-start | bytes 393220
  84.0 73.4 %all-gather.18.cloned.1.call-start = ((), (), s32[]{:S(2)}) async-start(), calls=%async_computation.6 | async-start | bytes 1310720 | tf_op jit(solution)/shard_map/all_gather | solution.py:191
  103.4 2.1 copy-start.2
  105.2 26.8 %copy-start.8 = (f32[96]{0:T(128)S(1)}, f32[96]{0:T(128)}, u32[]{:S(2)}) copy-start(f32[96]{0:T(128)} %param.34) | copy-start | bytes 1156
  106.7 27.1 %copy-start.10 = (f32[2]{0:T(128)S(1)}, f32[2]{0:T(128)}, u32[]{:S(2)}) copy-start(f32[2]{0:T(128)} %param.36) | copy-start | bytes 28
  106.8 83.2 %all-gather.16.cloned.1.call-start = ((), (), s32[]{:S(2)}) async-start(), calls=%async_computation.5 | async-start | bytes 1966080 | tf_op jit(solution)/shard_map/all_gather | solution.py:190
  132.3 0.7 copy-start.3
  133.1 111.0 %all-gather.20.cloned.1.call-start = ((), (), s32[]{:S(2)}) async-start(), calls=%async_computation.7 | async-start | bytes 4718592 | tf_op jit(solution)/shard_map/all_gather | solution.py:210
  191.5 52.5 %copy-start.1 = (bf16[128,2048]{1,0:T(8,128)(2,1)S(1)}, bf16[128,2048]{1,0:T(8,128)(2,1)}, u32[]{:S(2)}) copy-start(bf16[128,2048]{1,0:T(8,128)(2,1)} %param.20) | copy-start | bytes 1572868
  213.9 30.2 %all-to-all-start = ((bf16[8,128,128]{1,2,0:T(8,128)(2,1)}), bf16[8,128,128]{1,2,0:T(8,128)(2,1)S(1)}, u32[]{:S(2)}, u32[]{:S(2)}) async-start(bf16[8,128,128]{1,2,0:T(8,128)(2,1)} %copy.47), calls=%async_computation | async-start | bytes 524288 | tf_op jit(solution)/shard_map/all_to_all | solution.py:206
Sparse Core Ops, SparseCore 0:
  8.9 32.3 all-gather.7
  43.0 37.5 all-gather.9
  82.3 21.0 all-gather.13
  104.9 24.8 all-gather.11
  131.5 25.8 all-gather.17
  159.1 30.7 all-gather.15
  191.5 52.4 all-gather.19
where the time goes:
time: 256 us; the launch traced here: 255 us
  waiting for transfers between devices  125 us (49%)
  blocking collectives  56.2 us (22%)
  matrix products  33 us (13%)
  other arithmetic  14 us (5%)
  between operations  13.9 us (5%)
  local copies, waits for them, and re-layouts  7.88 us (3%)
  starting transfers between devices  4.82 us (2%)
    all_gather x1, waiting for transfers between devices, shards(): lax.all_gather(down_q, 'tp', axis=0, tiled=True)  33.1 us
    all_gather x1, waiting for transfers between devices, shards(): lax.all_gather(keys, 'sp', axis=0, tiled=True)  29.4 us
    all_gather x1, waiting for transfers between devices, shards(): lax.all_gather(out_weight, 'tp', axis=0, tiled=True)  25.6 us
    all_gather x1, waiting for transfers between devices, shards(): lax.all_gather(query_latent, 'tp', axis=0, tiled=True)  23 us
    all_gather x1, blocking collectives, shards(): modulations = lax.all_gather(summed, 'tp', axis=1, tiled=True)  14.7 us
    all_gather x1, blocking collectives, shards(): lax.all_gather(rope_rows[:own_rows], 'tp', axis=0, tiled=True)  13.1 us
    psum x1, blocking collectives, shards(): summed = lax.psum(partial_value, 'sp')  11.5 us
    dot_general x5, matrix products, absorb_block(): jnp.einsum('qhk,khd->qhd', weights.astype(jnp.bfloat16), value_block, pre...  10.7 us
  transfers between devices with their start and end apart: 8, of which 6 were waited for; matrix products, arithmetic and copies ran while one was open for 20% of the time, Pallas kernels for 0%

commit v1 on v0

v1 whole, which is shorter than its diff:
```python
import math

import jax
import jax.numpy as jnp
from jax import lax
from jax.experimental import pallas as pl
from jax.experimental.pallas import tpu as pltpu
from jax.sharding import PartitionSpec as P

NOPE = 64
ROPE = 32
VDIM = 64
GRID_W = 64
TOK_DEV = 1024
CTX_DEV = 32


epsilon = 1e-06
theta = 10000.0


def rms_scale(tensor, gain):
    return (
        tensor
        * lax.rsqrt(jnp.mean(tensor * tensor, axis=-1, keepdims=True) + epsilon)
        * gain.astype(jnp.float32)
    )


def axial_tables(positions):
    pair_count = ROPE // 4
    frequency = jnp.power(theta, -jnp.arange(pair_count, dtype=jnp.float32) / pair_count)
    row_angle = (positions // GRID_W).astype(jnp.float32)[:, None] * frequency
    col_angle = (positions % GRID_W).astype(jnp.float32)[:, None] * frequency
    return (jnp.cos(row_angle), jnp.sin(row_angle), jnp.cos(col_angle), jnp.sin(col_angle))


def rotate_half(tensor, cosine, sine_table):
    first, second = jnp.split(tensor, 2, axis=-1)
    cosine = cosine[:, None, :]
    sine_table = sine_table[:, None, :]
    return jnp.concatenate(
        [first * cosine - second * sine_table, second * cosine + first * sine_table], axis=-1
    )


def axial_rotate(tensor, tables):
    half_width = tensor.shape[-1] // 2
    return jnp.concatenate(
        [
            rotate_half(tensor[..., :half_width], tables[0], tables[1]),
            rotate_half(tensor[..., half_width:], tables[2], tables[3]),
        ],
        axis=-1,
    )


def modulate(row_block, gain, shifts, scales):
    normal = rms_scale(row_block.astype(jnp.float32), gain)
    return (normal * (1.0 + scales) + shifts).astype(jnp.bfloat16)


def make_queries(query_latent, up_query, query_gain, tables):
    amount = query_latent.shape[0]
    projected = jnp.dot(query_latent, up_query, preferred_element_type=jnp.float32).reshape(
        amount, -1, NOPE + ROPE
    )
    normal = rms_scale(projected, query_gain)
    return jnp.concatenate(
        [normal[..., :NOPE], axial_rotate(normal[..., NOPE:], tables)], axis=-1
    ).astype(jnp.bfloat16)


def make_keys(kv_latent, rope_rows, up_key, up_value, key_gain, tables):
    amount = kv_latent.shape[0]
    unrotated = jnp.dot(kv_latent, up_key, preferred_element_type=jnp.float32).reshape(
        amount, -1, NOPE
    )
    head_count = unrotated.shape[1]
    shared = jnp.broadcast_to(rope_rows.astype(jnp.float32)[:, None, :], (amount, head_count, ROPE))
    normal = rms_scale(jnp.concatenate([unrotated, shared], axis=-1), key_gain)
    if tables is not None:
        normal = jnp.concatenate(
            [normal[..., :NOPE], axial_rotate(normal[..., NOPE:], tables)], axis=-1
        )
    values = jnp.dot(kv_latent, up_value, preferred_element_type=jnp.float32).reshape(
        amount, head_count, VDIM
    )
    return (normal.astype(jnp.bfloat16), values.astype(jnp.bfloat16))


CORES = 2


def greet(sp_peers=True):
    sp, tp = lax.axis_index("sp"), lax.axis_index("tp")
    S, T = lax.axis_size("sp"), lax.axis_size("tp")
    barrier = pltpu.get_barrier_semaphore()
    for k in range(1, S):
        pl.semaphore_signal(barrier, inc=1, device_id={"sp": lax.rem(sp + k, S)}, device_id_type=pl.DeviceIdType.MESH)
    for k in range(1, T):
        pl.semaphore_signal(barrier, inc=1, device_id={"tp": lax.rem(tp + k, T)}, device_id_type=pl.DeviceIdType.MESH)
    pl.semaphore_wait(barrier, S + T - 2)


def remote(source, target, send, recv, device):
    return pltpu.make_async_remote_copy(
        src_ref=source,
        dst_ref=target,
        send_sem=send,
        recv_sem=recv,
        device_id=device,
        device_id_type=pl.DeviceIdType.MESH,
    )


class Line:
    def __init__(self, own, slots, send, recv, z, core, Z):
        self.own, self.slots, self.send, self.recv = own, slots, send, recv
        self.z, self.core, self.Z = z, core, Z

    def hop(self, block, step, first=False):
        to = lax.max(lax.min(self.z + step, self.Z - 1), 0)
        d = 0 if step > 0 else 1
        return remote(
            self.own if first else self.slots(block),
            self.slots(block),
            self.send.at[block, d],
            self.recv.at[block],
            {"tp": to * CORES + self.core},
        )

    def start(self):
        for step in (1, -1):
            ok = (self.z + step >= 0) & (self.z + step < self.Z)

            @pl.when(ok)
            def _():
                self.hop(self.z, step, True).start()

    def each(self, body):
        for k in range(1, self.Z):
            for step in (1, -1):
                block = self.z - step * k

                @pl.when((block >= 0) & (block < self.Z))
                def _():
                    body(block, step)

    def arrive(self, block, step):
        self.hop(block, step).wait_recv()
        ok = (self.z + step >= 0) & (self.z + step < self.Z)

        @pl.when(ok)
        def _():
            self.hop(block, step).start()

    def drain(self):
        for step in (1, -1):
            ok = (self.z + step >= 0) & (self.z + step < self.Z)

            @pl.when(ok)
            def _():
                self.hop(self.z, step, True).wait_send()

        def body(block, step):
            ok = (self.z + step >= 0) & (self.z + step < self.Z)

            @pl.when(ok)
            def _():
                self.hop(block, step).wait_send()

        self.each(body)


def loop(low, high, body):
    def step(k, carry):
        body(k)
        return carry

    lax.fori_loop(low, high, step, 0)


def weights_kernel(
    part, dq, dkv, ow, mods, dq_all, dkv_all, ow_part,
    pm, msum, m_send, m_recv, t_send, t_recv, l_send, l_recv, s_send, s_recv, c_send, c_recv, loc,
):
    sp, tp = lax.axis_index("sp"), lax.axis_index("tp")
    S, T = lax.axis_size("sp"), lax.axis_size("tp")
    Z = T // CORES
    z, core = tp // CORES, lax.rem(tp, CORES)
    mate = {"tp": tp + 1 - 2 * core}
    greet()
    downs = ((dq, dq_all), (dkv, dkv_all))

    def part_copy(k):
        return remote(part, pm.at[sp], m_send.at[k], m_recv.at[k], {"sp": lax.rem(sp + k, S)})

    loop(1, S, lambda k: part_copy(k).start())
    lines = [
        Line(a.at[sp], (lambda o: lambda b: o.at[b, core, sp])(o), l_send.at[i], l_recv.at[i], z, core, Z)
        for i, (a, o) in enumerate(downs)
    ]
    lines.append(Line(ow.at[sp], lambda b: ow_part.at[b], l_send.at[2], l_recv.at[2], z, core, Z))
    for line in lines[:2]:
        line.start()
    local = []
    for i, (a, o) in enumerate(downs):
        local.append(pltpu.make_async_copy(a, o.at[z, core], loc.at[i]))
    local.append(pltpu.make_async_copy(ow.at[sp], ow_part.at[z], loc.at[2]))
    for copy in local:
        copy.start()

    def mate_copy(i, block, own=False):
        a, o = downs[i]
        return remote(
            a if own else o.at[block, core], o.at[block, core], c_send.at[i, block], c_recv.at[i, block], mate
        )

    def mate_wait(i, block):
        a, o = downs[i]
        to = o.at[block, 1 - core]
        remote(to, to, c_send.at[i, block], c_recv.at[i, block], mate).wait_recv()

    for i in range(2):
        mate_copy(i, z, True).start()
    pm[sp] = part[...]
    loop(1, S, lambda k: part_copy(k).wait_recv())
    total = pm[0]
    for k in range(1, S):
        total = total + pm[k]
    msum[...] = total
    mods[tp] = total

    def spread(i, block, k):
        at = downs[i][1].at[block, core, sp]
        return remote(at, at, s_send.at[i, block, k], s_recv.at[i, block, k], {"sp": lax.rem(sp + k, S)})

    def gathered(i, block, k):
        at = downs[i][1].at[block, core, lax.rem(sp - k + S, S)]
        return remote(at, at, s_send.at[i, block, k], s_recv.at[i, block, k], {"sp": lax.rem(sp + k, S)})

    def body(block, step):
        for i in range(2):
            lines[i].arrive(block, step)
            loop(1, S, lambda k: spread(i, block, k).start())

    def mod_copy(k):
        return remote(msum, mods.at[tp], t_send.at[k], t_recv.at[k], {"tp": lax.rem(tp + k, T)})

    def mod_wait(k):
        to = mods.at[lax.rem(tp - k + T, T)]
        remote(msum, to, t_send.at[k], t_recv.at[k], {"tp": lax.rem(tp + k, T)}).wait_recv()

    loop(1, T, lambda k: mod_copy(k).start())
    lines[0].each(body)
    lines[2].start()
    lines[2].each(lines[2].arrive)

    def body(block, step):
        for i in range(2):
            loop(1, S, lambda k: gathered(i, block, k).wait_recv())
            mate_copy(i, block).start()

    lines[0].each(body)
    for copy in local:
        copy.wait()
    loop(1, T, mod_wait)
    for i in range(2):
        for b in range(Z):
            mate_wait(i, b)
    for i in range(2):
        mate_copy(i, z, True).wait_send()

    def body(block, step):
        for i in range(2):
            mate_copy(i, block).wait_send()
            loop(1, S, lambda k: spread(i, block, k).wait_send())

    lines[0].each(body)
    for line in lines:
        line.drain()
    loop(1, S, lambda k: part_copy(k).wait_send())
    loop(1, T, lambda k: mod_copy(k).wait_send())


def latents_kernel(lat, ow_part, lat_all, ow_all, l_send, l_recv, s_send, s_recv, c_send, c_recv, loc):
    sp, tp = lax.axis_index("sp"), lax.axis_index("tp")
    S, T = lax.axis_size("sp"), lax.axis_size("tp")
    Z = T // CORES
    z, core = tp // CORES, lax.rem(tp, CORES)
    mate = {"tp": tp + 1 - 2 * core}
    greet()
    line = Line(lat, lambda b: lat_all.at[b, core], l_send, l_recv, z, core, Z)
    line.start()

    def mate_copy(block, own=False):
        to = lat_all.at[block, core]
        return remote(lat if own else to, to, c_send.at[block], c_recv.at[block], mate)

    mate_copy(z, True).start()

    def spread(k):
        return remote(ow_part, ow_all.at[:, core, sp], s_send.at[k], s_recv.at[k], {"sp": lax.rem(sp + k, S)})

    def gathered(k):
        to = ow_all.at[:, core, lax.rem(sp - k + S, S)]
        return remote(ow_part, to, s_send.at[k], s_recv.at[k], {"sp": lax.rem(sp + k, S)})

    loop(1, S, lambda k: spread(k).start())
    own_lat = pltpu.make_async_copy(lat, lat_all.at[z, core], loc.at[0])
    own_ow = pltpu.make_async_copy(ow_part, ow_all.at[:, core, sp], loc.at[1])
    own_lat.start()
    own_ow.start()

    def body(block, step):
        line.arrive(block, step)
        mate_copy(block).start()

    line.each(body)
    own_lat.wait()
    own_ow.wait()
    loop(1, S, lambda k: gathered(k).wait_recv())
    whole = remote(ow_all.at[:, core], ow_all.at[:, core], c_send.at[Z], c_recv.at[Z], mate)
    whole.start()
    for b in range(Z):
        to = lat_all.at[b, 1 - core]
        remote(to, to, c_send.at[b], c_recv.at[b], mate).wait_recv()
    to = ow_all.at[:, 1 - core]
    remote(to, to, c_send.at[Z], c_recv.at[Z], mate).wait_recv()
    whole.wait_send()
    mate_copy(z, True).wait_send()
    line.each(lambda block, step: mate_copy(block).wait_send())
    line.drain()
    loop(1, S, lambda k: spread(k).wait_send())


def attend_kernel(
    q, kv, ctx, shift, out, kv_all, ctx_all, m_scr, l_scr, acc, att,
    k_send, k_recv, x_send, x_recv, a_send, a_recv,
):
    sp, tp = lax.axis_index("sp"), lax.axis_index("tp")
    S, T = lax.axis_size("sp"), lax.axis_size("tp")
    H, N, KD = q.shape
    rows = out.shape[1]
    TQ = math.gcd(N, 256)
    WIDE = KD + VDIM
    factor = KD ** (-0.5) * math.log2(math.e)
    greet()

    def ctx_copy(k):
        return remote(ctx, ctx_all.at[sp], x_send.at[k], x_recv.at[k], {"sp": lax.rem(sp + k, S)})

    def ctx_wait(k):
        to = ctx_all.at[lax.rem(sp - k + S, S)]
        remote(ctx, to, x_send.at[k], x_recv.at[k], {"sp": lax.rem(sp + k, S)}).wait_recv()

    def kv_copy(k):
        return remote(kv, kv_all.at[sp], k_send.at[k], k_recv.at[k], {"sp": lax.rem(sp + k, S)})

    loop(1, S, lambda k: ctx_copy(k).start())
    loop(1, S, lambda k: kv_copy(k).start())

    def lanes(p):
        total = p[:, :128]
        for j in range(1, p.shape[1] // 128):
            total = total + p[:, j * 128 : (j + 1) * 128]
        return total

    def first(qi):
        at = pl.ds(pl.multiple_of(qi * TQ, TQ), TQ)
        for h in range(H):
            kt = kv[h * WIDE : h * WIDE + KD, :]
            vt = kv[h * WIDE + KD : (h + 1) * WIDE, :]
            s = jnp.dot(q[h, at, :], kt, preferred_element_type=jnp.float32) * factor
            new = jnp.max(s, axis=1, keepdims=True)
            p = jnp.exp2(s - new)
            m_scr[h, at, :] = jnp.broadcast_to(new, (TQ, 128))
            l_scr[h, at, :] = lanes(p)
            acc[h, at, :] = lax.dot_general(
                p.astype(jnp.bfloat16), vt, (((1,), (1,)), ((), ())), preferred_element_type=jnp.float32
            )

    loop(0, N // TQ, first)

    def absorb(h, at, s, value, dims):
        old = m_scr[h, at, :][:, :1]
        new = jnp.maximum(old, jnp.max(s, axis=1, keepdims=True))
        scale = jnp.exp2(old - new)
        p = jnp.exp2(s - new)
        m_scr[h, at, :] = jnp.broadcast_to(new, (TQ, 128))
        l_scr[h, at, :] = l_scr[h, at, :] * scale + lanes(p)
        acc[h, at, :] = acc[h, at, :] * scale + lax.dot_general(
            p.astype(jnp.bfloat16), value, (dims, ((), ())), preferred_element_type=jnp.float32
        )

    ctx_all[sp] = ctx[...]
    loop(1, S, ctx_wait)

    def context_step(qi):
        at = pl.ds(pl.multiple_of(qi * TQ, TQ), TQ)
        for h in range(H):
            rows_all = ctx_all[...].reshape(-1, ctx_all.shape[2])
            kc = rows_all[:, h * 256 : h * 256 + 128][:, :KD]
            vc = rows_all[:, h * 256 + 128 : h * 256 + 256][:, :VDIM]
            s = lax.dot_general(q[h, at, :], kc, (((1,), (1,)), ((), ())), preferred_element_type=jnp.float32)
            s = s * factor + shift[h : h + 1, :1]
            absorb(h, at, s, vc, ((1,), (0,)))

    loop(0, N // TQ, context_step)

    def latent_step(k):
        slot = lax.rem(sp - k + S, S)
        to = kv_all.at[slot]
        remote(kv, to, k_send.at[k], k_recv.at[k], {"sp": lax.rem(sp + k, S)}).wait_recv()

        def tile(qi):
            at = pl.ds(pl.multiple_of(qi * TQ, TQ), TQ)
            for h in range(H):
                kt = kv_all[slot, h * WIDE : h * WIDE + KD, :]
                vt = kv_all[slot, h * WIDE + KD : (h + 1) * WIDE, :]
                s = jnp.dot(q[h, at, :], kt, preferred_element_type=jnp.float32) * factor
                absorb(h, at, s, vt, ((1,), (1,)))

        loop(0, N // TQ, tile)

    loop(1, S, latent_step)

    def finish(qi):
        at = pl.ds(pl.multiple_of(qi * TQ, TQ), TQ)
        heads = [acc[h, at, :] / jnp.sum(l_scr[h, at, :], axis=1, keepdims=True) for h in range(H)]
        att[at, :] = jnp.concatenate(heads, axis=1).astype(jnp.bfloat16)

    loop(0, N // TQ, finish)

    def give(k):
        peer = lax.rem(tp + k, T)
        return remote(
            att.at[pl.ds(pl.multiple_of(peer * rows, rows), rows)], out.at[tp], a_send.at[k], a_recv.at[k], {"tp": peer}
        )

    def take(k):
        to = out.at[lax.rem(tp - k + T, T)]
        remote(to, to, a_send.at[k], a_recv.at[k], {"tp": lax.rem(tp + k, T)}).wait_recv()

    loop(1, T, lambda k: give(k).start())
    out[tp] = att[pl.ds(pl.multiple_of(tp * rows, rows), rows), :]
    loop(1, T, take)
    loop(1, T, lambda k: give(k).wait_send())
    loop(1, S, lambda k: kv_copy(k).wait_send())
    loop(1, S, lambda k: ctx_copy(k).wait_send())


DMA = pltpu.SemaphoreType.DMA
VM = pl.BlockSpec(memory_space=pltpu.VMEM)
ANY = pl.BlockSpec(memory_space=pl.ANY)


def call(kernel, ident, outs, out_specs, scratch, args):
    return pl.pallas_call(
        kernel,
        out_shape=outs,
        in_specs=[VM] * len(args),
        out_specs=out_specs,
        scratch_shapes=scratch,
        compiler_params=pltpu.CompilerParams(
            collective_id=ident, has_side_effects=True, vmem_limit_bytes=48 * 1024 * 1024
        ),
    )(*args)


def rotated_columns(normal, tables):
    base = NOPE
    m = ROPE // 4
    a, b, c, d = (normal[..., base + i * m : base + (i + 1) * m, :] for i in range(4))
    rc, rs, cc, cs = (table.T for table in tables)
    return jnp.concatenate(
        [normal[..., :base, :], a * rc - b * rs, b * rc + a * rs, c * cc - d * cs, d * cc + c * cs], axis=-2
    )


def norm_columns(u, gain):
    return u * lax.rsqrt(jnp.mean(u * u, axis=-2, keepdims=True) + epsilon) * gain[:, None]


def shards(
    latent, context, cond, cond_context, mod_weight, norm_gain, down_q, down_kv, rope_weight, qlat_gain, kvlat_gain,
    up_query, up_key, up_value, query_gain, key_gain, context_bias, out_weight,
):
    seq_index = lax.axis_index("sp")
    S, T = lax.axis_size("sp"), lax.axis_size("tp")
    Z = T // CORES
    bf16, f32 = jnp.bfloat16, jnp.float32
    own_rows = latent.shape[0]
    block_tokens = own_rows * T
    row_span, cols = mod_weight.shape[1:]
    width = latent.shape[1]
    activated = jax.nn.silu(jnp.stack([cond, cond_context]).astype(f32)).astype(bf16)
    own_part = lax.dynamic_slice_in_dim(activated, seq_index * row_span, row_span, 1)
    both = jnp.einsum("cd,rde->rce", own_part, mod_weight, preferred_element_type=f32)
    partial_value = jnp.concatenate([both.reshape(6, cols), jnp.zeros((2, cols), f32)], axis=0)
    pieces = [w.reshape(S, w.shape[0] // S, w.shape[1]) for w in (down_q, down_kv, out_weight)]
    dq, dkv, ow = pieces
    mods, dq_all, dkv_all, ow_part = call(
        weights_kernel,
        1,
        (
            jax.ShapeDtypeStruct((T, 8, cols), f32),
            jax.ShapeDtypeStruct((Z, CORES) + dq.shape, bf16),
            jax.ShapeDtypeStruct((Z, CORES) + dkv.shape, bf16),
            jax.ShapeDtypeStruct((Z,) + ow.shape[1:], bf16),
        ),
        (VM, ANY, ANY, ANY),
        [
            pltpu.VMEM((S, 8, cols), f32), pltpu.VMEM((8, cols), f32),
            DMA((S,)), DMA((S,)), DMA((T,)), DMA((T,)),
            DMA((3, Z, 2)), DMA((3, Z)), DMA((2, Z, S)), DMA((2, Z, S)), DMA((2, Z)), DMA((2, Z)), DMA((3,)),
        ],
        (partial_value, dq, dkv, ow),
    )
    mods = mods.transpose(1, 0, 2).reshape(8, width)
    normed = modulate(latent, norm_gain, mods[0], mods[2])
    context_normed = modulate(context, norm_gain, mods[1], mods[3])
    gates = mods[4]
    stacked = jnp.concatenate([normed, context_normed], axis=0)
    query_down = jnp.dot(normed, dq_all.reshape(width, -1), preferred_element_type=f32)
    kv_down = jnp.dot(stacked, dkv_all.reshape(width, -1), preferred_element_type=f32)
    query_latent = rms_scale(query_down, qlat_gain).astype(bf16)
    kv_latent = rms_scale(kv_down, kvlat_gain).astype(bf16)
    rope_rows = jnp.dot(stacked, rope_weight, preferred_element_type=f32).astype(bf16)
    QR, KR = query_latent.shape[1], kv_latent.shape[1]
    lat = jnp.concatenate(
        [query_latent, kv_latent[:own_rows], jnp.pad(rope_rows[:own_rows], ((0, 0), (0, 128 - ROPE)))], axis=1
    )
    lat_all, ow_all = call(
        latents_kernel,
        2,
        (
            jax.ShapeDtypeStruct((Z, CORES) + lat.shape, bf16),
            jax.ShapeDtypeStruct((Z, CORES) + ow.shape, bf16),
        ),
        (ANY, ANY),
        [DMA((Z, 2)), DMA((Z,)), DMA((S,)), DMA((S,)), DMA((Z + 1,)), DMA((Z + 1,)), DMA((2,))],
        (lat, ow_part),
    )
    lat_all = lat_all.reshape(block_tokens, -1)
    ctx_keys, ctx_values = make_keys(
        kv_latent[own_rows:], rope_rows[own_rows:], up_key, up_value, key_gain, None
    )
    H = ctx_keys.shape[1]
    KD = NOPE + ROPE
    ctx = jnp.concatenate(
        [jnp.pad(ctx_keys, ((0, 0), (0, 0), (0, 128 - KD))), jnp.pad(ctx_values, ((0, 0), (0, 0), (0, 128 - VDIM)))],
        axis=-1,
    ).reshape(-1, H * 256)
    positions = seq_index * block_tokens + jnp.arange(block_tokens, dtype=jnp.int32)
    tables = axial_tables(positions)
    all_query, all_kv, all_rope = (
        lat_all[:, :QR], lat_all[:, QR : QR + KR], lat_all[:, QR + KR : QR + KR + ROPE]
    )
    uq = lax.dot_general(up_query, all_query, (((0,), (1,)), ((), ())), preferred_element_type=f32)
    queries = rotated_columns(norm_columns(uq.reshape(H, KD, -1), query_gain), tables).astype(bf16)
    queries = queries.transpose(0, 2, 1)
    uk = lax.dot_general(up_key, all_kv, (((0,), (1,)), ((), ())), preferred_element_type=f32)
    shared = jnp.broadcast_to(all_rope.astype(f32).T[None], (H, ROPE, block_tokens))
    keys = norm_columns(jnp.concatenate([uk.reshape(H, NOPE, -1), shared], axis=1), key_gain)
    keys = rotated_columns(keys, tables).astype(bf16)
    values = lax.dot_general(up_value, all_kv, (((0,), (1,)), ((), ())), preferred_element_type=f32).astype(bf16)
    kv = jnp.concatenate([keys, values.reshape(H, VDIM, -1)], axis=1).reshape(H * (KD + VDIM), -1)
    shift = (context_bias + math.log(TOK_DEV / CTX_DEV)) * math.log2(math.e)
    shift = jnp.broadcast_to(shift[:, None], (H, 128))
    token_rows = call(
        attend_kernel,
        3,
        jax.ShapeDtypeStruct((T, own_rows, H * VDIM), bf16),
        VM,
        [
            pltpu.VMEM((S,) + kv.shape, bf16), pltpu.VMEM((S,) + ctx.shape, bf16),
            pltpu.VMEM((H, block_tokens, 128), f32), pltpu.VMEM((H, block_tokens, 128), f32),
            pltpu.VMEM((H, block_tokens, VDIM), f32), pltpu.VMEM((block_tokens, H * VDIM), bf16),
            DMA((S,)), DMA((S,)), DMA((S,)), DMA((S,)), DMA((T,)), DMA((T,)),
        ],
        (queries, kv, ctx, shift),
    )
    token_rows = token_rows.transpose(1, 0, 2).reshape(own_rows, -1)
    projected = jnp.dot(token_rows, ow_all.reshape(-1, width), preferred_element_type=f32)
    return (latent.astype(f32) + gates * projected).astype(bf16)


def solution(mesh):
    in_specs = (
        P(("sp", "tp"), None),
        P("sp", None),
        P(),
        P(),
        P(None, "sp", "tp"),
        P(),
        P("tp", None),
        P("tp", None),
        P(),
        P(),
        P(),
        P(None, "tp"),
        P(None, "tp"),
        P(None, "tp"),
        P(),
        P(),
        P("tp"),
        P("tp", None),
    )
    out_specs = P(("sp", "tp"), None)
    return jax.shard_map(shards, mesh=mesh, in_specs=in_specs, out_specs=out_specs, check_vma=False)
```

time: 256 us -> 181 us (0.71)
  waiting for transfers between devices: 125 us -> 0 us
  Pallas kernels: 0 us -> 124 us
  blocking collectives: 56.2 us -> 0 us
  matrix products: 33 us -> 13 us
  local copies, waits for them, and re-layouts: 7.88 us -> 21.6 us
  between operations: 13.9 us -> 0.41 us
  other arithmetic: 14 us -> 21 us
  starting transfers between devices: 4.82 us -> 0 us
    pallas_call x0 -> x3, Pallas kernels: none -> 124 us  [call(): pl.pallas_call(kernel, out_shape=outs, in_specs=[VM] * len(args), out_spe...]
    all_gather x7 -> x0, waiting for transfers between devices: 122 us -> none  [the longest x1 33.1 us: shards(): lax.all_gather(down_q, 'tp', axis=0, tiled=True)]
    all_gather x4 -> x0, blocking collectives: 44.7 us -> none  [the longest x1 14.7 us: shards(): modulations = lax.all_gather(summed, 'tp', axis=1, tiled=True)]
    dot_general x17 -> x8, matrix products: 29.7 us -> 12.7 us  [the longest x1 3.73 us: shards(): jnp.dot(token_rows, ow_all.reshape(-1, width), preferred_element_type=f32)]
    psum x1 -> x0, blocking collectives: 11.5 us -> none  [shards(): summed = lax.psum(partial_value, 'sp')]
    concatenate x0 -> x4, local copies, waits for them, and re-layouts: none -> 8.53 us  [the longest x2 5.88 us: shards(): jnp.concatenate([keys, values.reshape(H, VDIM, -1)], axis=1)]
    reduce_sum x5 -> x2, other arithmetic: 5.68 us -> 0.73 us  [norm_columns(): jnp.mean(u * u, axis=-2, keepdims=True) + epsilon]
    all_to_all x1 -> x0, starting transfers between devices: 4.57 us -> none  [shards(): lax.all_to_all(attended, 'tp', split_axis=0, concat_axis=1, tiled=True)]
  transfers between devices with their start and end apart: 8 -> 0, of which waited for: 6 -> 0; matrix products, arithmetic and copies ran while one was open for 20% -> 0% of each run, Pallas kernels for 0% -> 0%
where the time goes in v1:
time: 181 us; the launch traced here: 180 us
  Pallas kernels  124 us (69%)
  local copies, waits for them, and re-layouts  21.6 us (12%)
  other arithmetic  21 us (12%)
  matrix products  13 us (7%)
    pallas_call x3, Pallas kernels, call(): pl.pallas_call(kernel, out_shape=outs, in_specs=[VM] * len(args), out_spe...  124 us
    concatenate x2, local copies, waits for them, and re-layouts, shards(): jnp.concatenate([keys, values.reshape(H, VDIM, -1)], axis=1)  5.88 us
    another operation x2, other arithmetic  4.44 us
    dot_general x1, matrix products, shards(): jnp.dot(token_rows, ow_all.reshape(-1, width), preferred_element_type=f32)  3.73 us

profile of v1, /device:TPU:0, one launch (start us, length us, event | category | flops | bytes accessed | tf_op | source)
XLA Modules:
  0.0 180.2 jit_solution(4576274301453639564)
XLA Ops:
  0.9 1.0 fusion.15
  2.5 1.2 fusion.4
  4.4 1.3 convert_element_type.91
  6.4 1.3 convert_element_type.85
  10.8 1.0 copy.29
  12.9 38.2 %shard_map.172 = (f32[8,8,256]{2,1,0:T(8,128)S(1)}, bf16[4,2,4,64,768]{4,3,2,1,0:T(8,128)(2,1)}, bf16[4,2,4,64,512]{4,3,2,1,0:T(8,128)(2,1)S(1)}, bf16[4,32,2048]{2,1,0:T(8,128)(2,1)S(1)}) custom-call(f32[8,256]{1,0:T(8,128)S(1)} %concatenate.28.part, bf16[4,64,768]{2,1,0:T(8,128)(2,1)S(1)} %bitcast.55, bf16[4,64,512]{2,1,0:T(8,128)(2,1)S(1)} %bitcast.56, ...), custom_call_target="tpu_custom_call" | custom-call | tf_op jit(solution)/shard_map/pallas_call | solution.py:460
  51.7 1.0 fusion.19
  53.8 2.6 %multiply_reduce_fusion.2 = (f32[128]{0:T(128)S(1)}, f32[128,768]{1,0:T(8,128)S(1)}) fusion(bf16[128,2048]{1,0:T(8,128)(2,1)S(1)} %fusion.8, bf16[2048,768]{1,0:T(8,128)(2,1)} %bitcast.63), kind=kOutput, calls=%fused_computation.40 | convolution fusion | flops 402849664 | bytes 4063744 | tf_op jit(solution)/shard_map/dot_general | solution.py:526
  61.3 34.6 %shard_map.173 = (bf16[4,2,128,1408]{3,2,1,0:T(8,128)(2,1)S(1)}, bf16[4,2,4,32,2048]{4,3,2,1,0:T(8,128)(2,1)}) custom-call(bf16[128,1408]{1,0:T(8,128)(2,1)S(1)} %fusion.14.lat, bf16[4,32,2048]{2,1,0:T(8,128)(2,1)S(1)} %get-tuple-element.14.ow_part), custom_call_target="tpu_custom_call" | custom-call | tf_op jit(solution)/shard_map/pallas_call | solution.py:460
  95.9 1.6 copy-done.1
  98.0 1.1 copy.34
  99.1 1.1 convert_bitcast_fusion
  100.3 2.5 %fusion.10 = f32[1024,128]{0,1:T(8,128)} fusion(bf16[512,128]{1,0:T(8,128)(2,1)S(1)} %copy-done.12, bf16[1024,1408]{1,0:T(8,128)(2,1)} %bitcast.52), kind=kOutput, calls=%fused_computation.31 | convolution fusion | flops 134217728 | bytes 1703936 | tf_op jit(solution)/shard_map/dot_general | solution.py:564
  102.8 1.6 fusion.2
  104.6 1.3 copy.28
  105.9 1.4 copy.33
  108.0 2.2 %multiply_multiply_fusion = (f32[2,96,1024]{1,2,0:T(8,128)S(1)}, f32[2,96,1024]{1,2,0:T(8,128)S(1)}) fusion(f32[2,32,1024]{1,2,0:T(8,128)S(1)} %broadcast_in_dim.6, f32[2,64,1024]{1,2,0:T(8,128)S(1)} %copy.33, f32[96]{0:T(128)S(1)} %copy-done.16, f32[2,1024]{1,0:T(2,128)S(1)} %add_rsqrt_fusion.1, f32[96]{0:T(128)S(1)} %copy-done.17, ...), kind=kLoop, calls=%fused_computation.23 | loop fusion | flops 983040 | bytes 3162880 | tf_op jit(solution)/shard_map/mul | solution.py:483
  111.9 2.9 %add_convert_fusion = (bf16[2,8,1024]{1,2,0:T(8,128)(2,1)}, bf16[2,8,1024]{1,2,0:T(8,128)(2,1)}, bf16[2,8,1024]{1,2,0:T(8,128)(2,1)S(1)}, bf16[2,8,1024]{1,2,0:T...) fusion(f32[2,96,1024]{1,2,0:T(8,128)S(1)} %get-tuple-element.46, ...), kind=kLoop, calls=%fused_computation.19 | loop fusion | flops 393216 | bytes 720896 | tf_op jit(solution)/shard_map/convert.5
  114.8 1.6 add_convert_fusion.1
  116.4 2.6 %concatenate.31 = bf16[2,96,1024]{1,2,0:T(8,128)(2,1)S(1)} concatenate(bf16[2,64,1024]{1,2,0:T(8,128)(2,1)} %slice.150, bf16[2,8,1024]{1,2,0:T(8,128)(2,1)S(1)} %get-tuple-element.27, bf16[2,8,1024]{1,2,0:T(8,128)(2,1)S(1)} %copy-done.11, bf16[2,8,1024]{1,2,0:T(8,128)(2,1)S(1)} %get-tuple-element.25, bf16[2,8,1024]{1,2,0:T(8,128)(2,1)S(1)} %get-tuple-element.26), dimensions={1} | concatenate | bytes 786432 | tf_op jit(solution)/shard_map/concatenate | solution.py:477
  119.0 4.4 %concatenate.33 = bf16[2,160,1024]{1,2,0:T(8,128)(2,1)} concatenate(bf16[2,64,1024]{1,2,0:T(8,128)(2,1)} %slice.149, bf16[2,8,1024]{1,2,0:T(8,128)(2,1)} %get-tuple-element.20, bf16[2,8,1024]{1,2,0:T(8,128)(2,1)} %get-tuple-element.19, bf16[2,8,1024]{1,2,0:T(8,128)(2,1)} %get-tuple-element.18, bf16[2,8,1024]{1,2,0:T(8,128)(2,1)} %get-tuple-element.17, bf16[2,64,1024]{1,2,0:T(8,128)(2,1)} %copy.34), dimensions={1} | concatenate | bytes 1310720 | tf_op jit(solution)/shard_map/concatenate | solution.py:569
  123.4 1.5 copy.35
  124.9 51.3 %shard_map.174 = bf16[8,128,128]{2,1,0:T(8,128)(2,1)S(1)} custom-call(bf16[2,1024,96]{2,1,0:T(8,128)(2,1)S(1)} %bitcast.48, bf16[320,1024]{1,0:T(8,128)(2,1)S(1)} %bitcast.47, bf16[32,512]{1,0:T(8,128)(2,1)S(1)} %bitcast.57, f32[2,128]{1,0:T(2,128)S(1)} %broadcast_in_dim.8.shift), custom_call_target="tpu_custom_call" | custom-call | tf_op jit(solution)/shard_map/pallas_call | solution.py:460
  176.4 3.7 %fusion.1 = bf16[128,2048]{1,0:T(8,128)(2,1)} fusion(bf16[128,1024]{0,1:T(8,128)(2,1)S(1)} %bitcast.65, bf16[1024,2048]{1,0:T(8,128)(2,1)} %bitcast.60, bf16[128,2048]{1,0:T(8,128)(2,1)S(1)} %copy-done.9, f32[2048]{0:T(1024)S(1)} %bitcast.68), kind=kOutput, calls=%fused_computation.2 | convolution fusion | flops 537919488 | bytes 5513216 | tf_op jit(solution)/shard_map/dot_general | solution.py:586
  (85 shorter events, 16.6 us)
Async XLA Ops:
  0.0 9.1 %copy-start = (bf16[3,512,256]{2,1,0:T(8,128)(2,1)S(1)}, bf16[3,512,256]{2,1,0:T(8,128)(2,1)}, u32[]{:S(2)}) copy-start(bf16[3,512,256]{2,1,0:T(8,128)(2,1)} %param.22) | copy-start | bytes 2359300
  0.0 52.8 %copy-start.8 = (bf16[128,2048]{1,0:T(8,128)(2,1)S(1)}, bf16[128,2048]{1,0:T(8,128)(2,1)}, u32[]{:S(2)}) copy-start(bf16[128,2048]{1,0:T(8,128)(2,1)} %param.18) | copy-start | bytes 1572868
  0.0 12.9 %copy-start.3 = (bf16[128,2048]{1,0:T(8,128)(2,1)S(1)}, bf16[128,2048]{1,0:T(8,128)(2,1)}, u32[]{:S(2)}) copy-start(bf16[128,2048]{1,0:T(8,128)(2,1)} %param.35) | copy-start | bytes 1572868
  0.0 12.9 %copy-start.5 = (bf16[256,512]{1,0:T(8,128)(2,1)S(1)}, bf16[256,512]{1,0:T(8,128)(2,1)}, u32[]{:S(2)}) copy-start(bf16[256,512]{1,0:T(8,128)(2,1)} %param.25) | copy-start | bytes 786436
  0.0 12.9 %copy-start.4 = (bf16[256,768]{1,0:T(8,128)(2,1)S(1)}, bf16[256,768]{1,0:T(8,128)(2,1)}, u32[]{:S(2)}) copy-start(bf16[256,768]{1,0:T(8,128)(2,1)} %param.24) | copy-start | bytes 1179652
  53.8 3.3 %copy-start.18 = (bf16[2048,32]{0,1:T(8,128)(2,1)S(1)}, bf16[2048,32]{0,1:T(8,128)(2,1)}, u32[]{:S(2)}) copy-start(bf16[2048,32]{0,1:T(8,128)(2,1)} %param.26) | copy-start | bytes 393220
  56.4 1.6 copy-start.15
  56.4 1.8 %copy-start.13 = (bf16[512,128]{1,0:T(8,128)(2,1)S(1)}, bf16[512,128]{1,0:T(8,128)(2,1)}, u32[]{:S(2)}) copy-start(bf16[512,128]{1,0:T(8,128)(2,1)} %param.31) | copy-start | bytes 393220
  56.4 2.1 %copy-start.12 = (bf16[512,128]{1,0:T(8,128)(2,1)S(1)}, bf16[512,128]{1,0:T(8,128)(2,1)}, u32[]{:S(2)}) copy-start(bf16[512,128]{1,0:T(8,128)(2,1)} %param.30) | copy-start | bytes 393220
  95.9 1.6 copy-start.1
  99.1 3.7 %copy-start.2 = (bf16[4,2,128,1408]{3,2,1,0:T(8,128)(2,1)S(1)}, bf16[4,2,128,1408]{3,2,1,0:T(8,128)(2,1)}, u32[]{:S(2)}) copy-start(bf16[4,2,128,1408]{3,2,1,0:T(8,128)(2,1)} %copy-done.1) | copy-start | bytes 8650756
  104.5 3.4 %copy-start.16 = (f32[96]{0:T(128)S(1)}, f32[96]{0:T(128)}, u32[]{:S(2)}) copy-start(f32[96]{0:T(128)} %param.33) | copy-start | bytes 1156
  104.5 3.4 %copy-start.17 = (f32[96]{0:T(128)S(1)}, f32[96]{0:T(128)}, u32[]{:S(2)}) copy-start(f32[96]{0:T(128)} %param.32) | copy-start | bytes 1156
  107.9 4.0 %copy-start.6 = (f32[8,1024]{0,1:T(8,128)S(1)}, f32[8,1024]{0,1:T(8,128)}, u32[]{:S(2)}) copy-start(f32[8,1024]{0,1:T(8,128)} %copy.30) | copy-start | bytes 98308
  108.0 4.0 %copy-start.7 = (f32[8,1024]{0,1:T(8,128)S(1)}, f32[8,1024]{0,1:T(8,128)}, u32[]{:S(2)}) copy-start(f32[8,1024]{0,1:T(8,128)} %copy.29) | copy-start | bytes 98308
  108.0 4.0 %copy-start.10 = (f32[8,1024]{0,1:T(8,128)S(1)}, f32[8,1024]{0,1:T(8,128)}, u32[]{:S(2)}) copy-start(f32[8,1024]{0,1:T(8,128)} %copy.32) | copy-start | bytes 98308
  114.8 1.6 copy-start.11
  123.4 53.0 %copy-start.9 = (bf16[128,2048]{1,0:T(8,128)(2,1)S(1)}, bf16[128,2048]{1,0:T(8,128)(2,1)}, u32[]{:S(2)}) copy-start(bf16[128,2048]{1,0:T(8,128)(2,1)} %param.18) | copy-start | bytes 1572868
  123.4 53.0 %copy-start.14 = (f32[1,8,256]{2,0,1:T(1,128)S(1)}, f32[1,8,256]{2,0,1:T(1,128)}, u32[]{:S(2)}) copy-start(f32[1,8,256]{2,0,1:T(1,128)} %get-tuple-element.29) | copy-start | bytes 24580

commit v2 on v1

--- a/solution.py
+++ b/solution.py
@@ -182,7 +182,7 @@
 
 
 def weights_kernel(
-    part, dq, dkv, ow, mods, dq_all, dkv_all, ow_part,
+    act, mod_weight, dq, dkv, ow, mods, dq_all, dkv_all, ow_part,
     pm, msum, m_send, m_recv, t_send, t_recv, l_send, l_recv, s_send, s_recv, c_send, c_recv, loc,
 ):
     sp, tp = lax.axis_index("sp"), lax.axis_index("tp")
@@ -190,13 +190,14 @@
     Z = T // CORES
     z, core = tp // CORES, lax.rem(tp, CORES)
     mate = {"tp": tp + 1 - 2 * core}
+    for r in range(mod_weight.shape[0]):
+        pm[sp, r * 8 : (r + 1) * 8, :] = jnp.dot(act[...], mod_weight[r], preferred_element_type=jnp.float32)
     greet()
     downs = ((dq, dq_all), (dkv, dkv_all))
 
     def part_copy(k):
-        return remote(part, pm.at[sp], m_send.at[k], m_recv.at[k], {"sp": lax.rem(sp + k, S)})
-
-    loop(1, S, lambda k: part_copy(k).start())
+        return remote(pm.at[sp], pm.at[sp], m_send.at[k], m_recv.at[k], {"sp": lax.rem(sp + k, S)})
+
     lines = [
         Line(a.at[sp], (lambda o: lambda b: o.at[b, core, sp])(o), l_send.at[i], l_recv.at[i], z, core, Z)
         for i, (a, o) in enumerate(downs)
@@ -204,6 +205,7 @@
     lines.append(Line(ow.at[sp], lambda b: ow_part.at[b], l_send.at[2], l_recv.at[2], z, core, Z))
     for line in lines[:2]:
         line.start()
+    loop(1, S, lambda k: part_copy(k).start())
     local = []
     for i, (a, o) in enumerate(downs):
         local.append(pltpu.make_async_copy(a, o.at[z, core], loc.at[i]))
@@ -224,8 +226,12 @@
 
     for i in range(2):
         mate_copy(i, z, True).start()
-    pm[sp] = part[...]
-    loop(1, S, lambda k: part_copy(k).wait_recv())
+
+    def part_wait(k):
+        to = pm.at[lax.rem(sp - k + S, S)]
+        remote(to, to, m_send.at[k], m_recv.at[k], {"sp": lax.rem(sp + k, S)}).wait_recv()
+
+    loop(1, S, part_wait)
     total = pm[0]
     for k in range(1, S):
         total = total + pm[k]
@@ -284,69 +290,44 @@
     loop(1, T, lambda k: mod_copy(k).wait_send())
 
 
-def latents_kernel(lat, ow_part, lat_all, ow_all, l_send, l_recv, s_send, s_recv, c_send, c_recv, loc):
+def attend_kernel(
+    lat_kv, lat_q, ow_part, ctx, shift, uq, ukv, pick, gain_q, gain_k, tables,
+    out, ow_all,
+    kv_lats, q_lats, q, kv, kv_all, ctx_all, m_scr, l_scr, acc, att,
+    l_send, l_recv, c_send, c_recv, s_send, s_recv,
+    k_send, k_recv, x_send, x_recv, a_send, a_recv, loc,
+):
     sp, tp = lax.axis_index("sp"), lax.axis_index("tp")
     S, T = lax.axis_size("sp"), lax.axis_size("tp")
     Z = T // CORES
     z, core = tp // CORES, lax.rem(tp, CORES)
     mate = {"tp": tp + 1 - 2 * core}
-    greet()
-    line = Line(lat, lambda b: lat_all.at[b, core], l_send, l_recv, z, core, Z)
-    line.start()
-
-    def mate_copy(block, own=False):
-        to = lat_all.at[block, core]
-        return remote(lat if own else to, to, c_send.at[block], c_recv.at[block], mate)
-
-    mate_copy(z, True).start()
-
-    def spread(k):
-        return remote(ow_part, ow_all.at[:, core, sp], s_send.at[k], s_recv.at[k], {"sp": lax.rem(sp + k, S)})
-
-    def gathered(k):
-        to = ow_all.at[:, core, lax.rem(sp - k + S, S)]
-        return remote(ow_part, to, s_send.at[k], s_recv.at[k], {"sp": lax.rem(sp + k, S)})
-
-    loop(1, S, lambda k: spread(k).start())
-    own_lat = pltpu.make_async_copy(lat, lat_all.at[z, core], loc.at[0])
-    own_ow = pltpu.make_async_copy(ow_part, ow_all.at[:, core, sp], loc.at[1])
-    own_lat.start()
-    own_ow.start()
-
-    def body(block, step):
-        line.arrive(block, step)
-        mate_copy(block).start()
-
-    line.each(body)
-    own_lat.wait()
-    own_ow.wait()
-    loop(1, S, lambda k: gathered(k).wait_recv())
-    whole = remote(ow_all.at[:, core], ow_all.at[:, core], c_send.at[Z], c_recv.at[Z], mate)
-    whole.start()
-    for b in range(Z):
-        to = lat_all.at[b, 1 - core]
-        remote(to, to, c_send.at[b], c_recv.at[b], mate).wait_recv()
-    to = ow_all.at[:, 1 - core]
-    remote(to, to, c_send.at[Z], c_recv.at[Z], mate).wait_recv()
-    whole.wait_send()
-    mate_copy(z, True).wait_send()
-    line.each(lambda block, step: mate_copy(block).wait_send())
-    line.drain()
-    loop(1, S, lambda k: spread(k).wait_send())
-
-
-def attend_kernel(
-    q, kv, ctx, shift, out, kv_all, ctx_all, m_scr, l_scr, acc, att,
-    k_send, k_recv, x_send, x_recv, a_send, a_recv,
-):
-    sp, tp = lax.axis_index("sp"), lax.axis_index("tp")
-    S, T = lax.axis_size("sp"), lax.axis_size("tp")
-    H, N, KD = q.shape
+    H, N, _ = q.shape
     rows = out.shape[1]
+    span = rows * CORES
+    KD = NOPE + ROPE
     TQ = math.gcd(N, 256)
     WIDE = KD + VDIM
     factor = KD ** (-0.5) * math.log2(math.e)
     greet()
+    lats = ((lat_kv, kv_lats), (lat_q, q_lats))
+    lines = [
+        Line(own, (lambda o: lambda b: o.at[b, core])(every), l_send.at[i], l_recv.at[i], z, core, Z)
+        for i, (own, every) in enumerate(lats)
+    ]
+
+    def mate_copy(i, block, own=False):
+        to = lats[i][1].at[block, core]
+        return remote(lats[i][0] if own else to, to, c_send.at[i, block], c_recv.at[i, block], mate)
+
+    def mate_wait(i, block):
+        to = lats[i][1].at[block, 1 - core]
+        remote(to, to, c_send.at[i, block], c_recv.at[i, block], mate).wait_recv()
+
+    lines[0].start()
+    mate_copy(0, z, True).start()
+    lines[1].start()
+    mate_copy(1, z, True).start()
 
     def ctx_copy(k):
         return remote(ctx, ctx_all.at[sp], x_send.at[k], x_recv.at[k], {"sp": lax.rem(sp + k, S)})
@@ -358,8 +339,69 @@
     def kv_copy(k):
         return remote(kv, kv_all.at[sp], k_send.at[k], k_recv.at[k], {"sp": lax.rem(sp + k, S)})
 
+    def spread(k):
+        return remote(ow_part, ow_all.at[:, core, sp], s_send.at[k], s_recv.at[k], {"sp": lax.rem(sp + k, S)})
+
+    def gathered(k):
+        to = ow_all.at[:, core, lax.rem(sp - k + S, S)]
+        return remote(ow_part, to, s_send.at[k], s_recv.at[k], {"sp": lax.rem(sp + k, S)})
+
     loop(1, S, lambda k: ctx_copy(k).start())
+    loop(1, S, lambda k: spread(k).start())
+    own_ow = pltpu.make_async_copy(ow_part, ow_all.at[:, core, sp], loc)
+    own_ow.start()
+    ctx_all[sp] = ctx[...]
+    kv_lats[z, core] = lat_kv[...]
+    q_lats[z, core] = lat_q[...]
+
+    NT = (((1,), (1,)), ((), ()))
+
+    def turned(u, gain, at):
+        u = u * lax.rsqrt(jnp.mean(u * u, axis=0, keepdims=True) + epsilon) * gain[:, :1]
+        m = ROPE // 4
+        a, b, c, d = (u[NOPE + i * m : NOPE + (i + 1) * m, :] for i in range(4))
+        rc, rs, cc, cs = (tables[i, :, at] for i in range(4))
+        return jnp.concatenate(
+            [u[:NOPE, :], a * rc - b * rs, b * rc + a * rs, c * cc - d * cs, d * cc + c * cs], axis=0
+        )
+
+    def passed(i):
+        def body(block, step):
+            lines[i].arrive(block, step)
+            mate_copy(i, block).start()
+
+        lines[i].each(body)
+
+    passed(0)
+    rank = ukv.shape[1]
+
+    def expand_kv(b):
+        mate_wait(0, b)
+        at = pl.ds(pl.multiple_of(b * span, span), span)
+        rows_in = kv_lats[b].reshape(span, kv_lats.shape[3])
+        u = lax.dot_general(ukv[...], rows_in[:, :rank], NT, preferred_element_type=jnp.float32)
+        rope = lax.dot_general(pick[...], rows_in[:, rank:], NT, preferred_element_type=jnp.float32)
+        for h in range(H):
+            key = turned(jnp.concatenate([u[h * NOPE : (h + 1) * NOPE, :], rope], axis=0), gain_k[...], at)
+            kv[h * WIDE : h * WIDE + KD, at] = key.astype(jnp.bfloat16)
+            base = H * NOPE + h * VDIM
+            kv[h * WIDE + KD : (h + 1) * WIDE, at] = u[base : base + VDIM, :].astype(jnp.bfloat16)
+
+    loop(0, Z, expand_kv)
     loop(1, S, lambda k: kv_copy(k).start())
+    passed(1)
+
+    def expand_q(b):
+        mate_wait(1, b)
+        at = pl.ds(pl.multiple_of(b * span, span), span)
+        rows_in = q_lats[b].reshape(span, q_lats.shape[3])
+        u = lax.dot_general(uq[...], rows_in, NT, preferred_element_type=jnp.float32)
+        for h in range(H):
+            query = turned(u[h * KD : (h + 1) * KD, :], gain_q[...], at)
+            query = jnp.concatenate([query, jnp.zeros((128 - KD, span), jnp.float32)], axis=0)
+            q[h, at, :] = query.T.astype(jnp.bfloat16)
+
+    loop(0, Z, expand_q)
 
     def lanes(p):
         total = p[:, :128]
@@ -372,14 +414,12 @@
         for h in range(H):
             kt = kv[h * WIDE : h * WIDE + KD, :]
             vt = kv[h * WIDE + KD : (h + 1) * WIDE, :]
-            s = jnp.dot(q[h, at, :], kt, preferred_element_type=jnp.float32) * factor
+            s = jnp.dot(q[h, at, :][:, :KD], kt, preferred_element_type=jnp.float32) * factor
             new = jnp.max(s, axis=1, keepdims=True)
             p = jnp.exp2(s - new)
             m_scr[h, at, :] = jnp.broadcast_to(new, (TQ, 128))
             l_scr[h, at, :] = lanes(p)
-            acc[h, at, :] = lax.dot_general(
-                p.astype(jnp.bfloat16), vt, (((1,), (1,)), ((), ())), preferred_element_type=jnp.float32
-            )
+            acc[h, at, :] = lax.dot_general(p.astype(jnp.bfloat16), vt, NT, preferred_element_type=jnp.float32)
 
     loop(0, N // TQ, first)
 
@@ -394,7 +434,6 @@
             p.astype(jnp.bfloat16), value, (dims, ((), ())), preferred_element_type=jnp.float32
         )
 
-    ctx_all[sp] = ctx[...]
     loop(1, S, ctx_wait)
 
     def context_step(qi):
@@ -403,7 +442,7 @@
             rows_all = ctx_all[...].reshape(-1, ctx_all.shape[2])
             kc = rows_all[:, h * 256 : h * 256 + 128][:, :KD]
             vc = rows_all[:, h * 256 + 128 : h * 256 + 256][:, :VDIM]
-            s = lax.dot_general(q[h, at, :], kc, (((1,), (1,)), ((), ())), preferred_element_type=jnp.float32)
+            s = lax.dot_general(q[h, at, :][:, :KD], kc, (((1,), (1,)), ((), ())), preferred_element_type=jnp.float32)
             s = s * factor + shift[h : h + 1, :1]
             absorb(h, at, s, vc, ((1,), (0,)))
 
@@ -419,11 +458,16 @@
             for h in range(H):
                 kt = kv_all[slot, h * WIDE : h * WIDE + KD, :]
                 vt = kv_all[slot, h * WIDE + KD : (h + 1) * WIDE, :]
-                s = jnp.dot(q[h, at, :], kt, preferred_element_type=jnp.float32) * factor
+                s = jnp.dot(q[h, at, :][:, :KD], kt, preferred_element_type=jnp.float32) * factor
                 absorb(h, at, s, vt, ((1,), (1,)))
 
         loop(0, N // TQ, tile)
 
+    own_ow.wait()
+    loop(1, S, lambda k: gathered(k).wait_recv())
+    half = ow_all.at[:, core]
+    whole = remote(half, half, c_send.at[0, Z], c_recv.at[0, Z], mate)
+    whole.start()
     loop(1, S, latent_step)
 
     def finish(qi):
@@ -449,6 +493,14 @@
     loop(1, T, lambda k: give(k).wait_send())
     loop(1, S, lambda k: kv_copy(k).wait_send())
     loop(1, S, lambda k: ctx_copy(k).wait_send())
+    loop(1, S, lambda k: spread(k).wait_send())
+    to = ow_all.at[:, 1 - core]
+    remote(to, to, c_send.at[0, Z], c_recv.at[0, Z], mate).wait_recv()
+    whole.wait_send()
+    for i in range(2):
+        mate_copy(i, z, True).wait_send()
+        lines[i].each(lambda block, step: mate_copy(i, block).wait_send())
+        lines[i].drain()
 
 
 DMA = pltpu.SemaphoreType.DMA
@@ -467,20 +519,6 @@
             collective_id=ident, has_side_effects=True, vmem_limit_bytes=48 * 1024 * 1024
         ),
     )(*args)
-
-
-def rotated_columns(normal, tables):
-    base = NOPE
-    m = ROPE // 4
-    a, b, c, d = (normal[..., base + i * m : base + (i + 1) * m, :] for i in range(4))
-    rc, rs, cc, cs = (table.T for table in tables)
-    return jnp.concatenate(
-        [normal[..., :base, :], a * rc - b * rs, b * rc + a * rs, c * cc - d * cs, d * cc + c * cs], axis=-2
-    )
-
-
-def norm_columns(u, gain):
-    return u * lax.rsqrt(jnp.mean(u * u, axis=-2, keepdims=True) + epsilon) * gain[:, None]
 
 
 def shards(
@@ -497,31 +535,30 @@
     width = latent.shape[1]
     activated = jax.nn.silu(jnp.stack([cond, cond_context]).astype(f32)).astype(bf16)
     own_part = lax.dynamic_slice_in_dim(activated, seq_index * row_span, row_span, 1)
-    both = jnp.einsum("cd,rde->rce", own_part, mod_weight, preferred_element_type=f32)
-    partial_value = jnp.concatenate([both.reshape(6, cols), jnp.zeros((2, cols), f32)], axis=0)
+    act = jnp.concatenate([own_part, jnp.zeros((6, row_span), bf16)], axis=0)
     pieces = [w.reshape(S, w.shape[0] // S, w.shape[1]) for w in (down_q, down_kv, out_weight)]
     dq, dkv, ow = pieces
     mods, dq_all, dkv_all, ow_part = call(
         weights_kernel,
         1,
         (
-            jax.ShapeDtypeStruct((T, 8, cols), f32),
+            jax.ShapeDtypeStruct((T, 24, cols), f32),
             jax.ShapeDtypeStruct((Z, CORES) + dq.shape, bf16),
             jax.ShapeDtypeStruct((Z, CORES) + dkv.shape, bf16),
             jax.ShapeDtypeStruct((Z,) + ow.shape[1:], bf16),
         ),
         (VM, ANY, ANY, ANY),
         [
-            pltpu.VMEM((S, 8, cols), f32), pltpu.VMEM((8, cols), f32),
+            pltpu.VMEM((S, 24, cols), f32), pltpu.VMEM((24, cols), f32),
             DMA((S,)), DMA((S,)), DMA((T,)), DMA((T,)),
             DMA((3, Z, 2)), DMA((3, Z)), DMA((2, Z, S)), DMA((2, Z, S)), DMA((2, Z)), DMA((2, Z)), DMA((3,)),
         ],
-        (partial_value, dq, dkv, ow),
-    )
-    mods = mods.transpose(1, 0, 2).reshape(8, width)
-    normed = modulate(latent, norm_gain, mods[0], mods[2])
-    context_normed = modulate(context, norm_gain, mods[1], mods[3])
-    gates = mods[4]
+        (act, mod_weight, dq, dkv, ow),
+    )
+    mods = mods.transpose(1, 0, 2).reshape(24, width)
+    normed = modulate(latent, norm_gain, mods[0], mods[8])
+    context_normed = modulate(context, norm_gain, mods[1], mods[9])
+    gates = mods[16]
     stacked = jnp.concatenate([normed, context_normed], axis=0)
     query_down = jnp.dot(normed, dq_all.reshape(width, -1), preferred_element_type=f32)
     kv_down = jnp.dot(stacked, dkv_all.reshape(width, -1), preferred_element_type=f32)
@@ -529,21 +566,9 @@
     kv_latent = rms_scale(kv_down, kvlat_gain).astype(bf16)
     rope_rows = jnp.dot(stacked, rope_weight, preferred_element_type=f32).astype(bf16)
     QR, KR = query_latent.shape[1], kv_latent.shape[1]
-    lat = jnp.concatenate(
-        [query_latent, kv_latent[:own_rows], jnp.pad(rope_rows[:own_rows], ((0, 0), (0, 128 - ROPE)))], axis=1
-    )
-    lat_all, ow_all = call(
-        latents_kernel,
-        2,
-        (
-            jax.ShapeDtypeStruct((Z, CORES) + lat.shape, bf16),
-            jax.ShapeDtypeStruct((Z, CORES) + ow.shape, bf16),
-        ),
-        (ANY, ANY),
-        [DMA((Z, 2)), DMA((Z,)), DMA((S,)), DMA((S,)), DMA((Z + 1,)), DMA((Z + 1,)), DMA((2,))],
-        (lat, ow_part),
-    )
-    lat_all = lat_all.reshape(block_tokens, -1)
+    lat_kv = jnp.concatenate(
+        [kv_latent[:own_rows], jnp.pad(rope_rows[:own_rows], ((0, 0), (0, 128 - ROPE)))], axis=1
+    )
     ctx_keys, ctx_values = make_keys(
         kv_latent[own_rows:], rope_rows[own_rows:], up_key, up_value, key_gain, None
     )
@@ -555,32 +580,33 @@
     ).reshape(-1, H * 256)
     positions = seq_index * block_tokens + jnp.arange(block_tokens, dtype=jnp.int32)
     tables = axial_tables(positions)
-    all_query, all_kv, all_rope = (
-        lat_all[:, :QR], lat_all[:, QR : QR + KR], lat_all[:, QR + KR : QR + KR + ROPE]
-    )
-    uq = lax.dot_general(up_query, all_query, (((0,), (1,)), ((), ())), preferred_element_type=f32)
-    queries = rotated_columns(norm_columns(uq.reshape(H, KD, -1), query_gain), tables).astype(bf16)
-    queries = queries.transpose(0, 2, 1)
-    uk = lax.dot_general(up_key, all_kv, (((0,), (1,)), ((), ())), preferred_element_type=f32)
-    shared = jnp.broadcast_to(all_rope.astype(f32).T[None], (H, ROPE, block_tokens))
-    keys = norm_columns(jnp.concatenate([uk.reshape(H, NOPE, -1), shared], axis=1), key_gain)
-    keys = rotated_columns(keys, tables).astype(bf16)
-    values = lax.dot_general(up_value, all_kv, (((0,), (1,)), ((), ())), preferred_element_type=f32).astype(bf16)
-    kv = jnp.concatenate([keys, values.reshape(H, VDIM, -1)], axis=1).reshape(H * (KD + VDIM), -1)
+    tables = jnp.stack([table.T for table in tables])
+    uq = up_query.T
+    ukv = jnp.concatenate([up_key, up_value], axis=1).T
+    pick = jnp.eye(ROPE, 128, dtype=bf16)
+    gain_q = jnp.broadcast_to(query_gain[:, None], (KD, 128))
+    gain_k = jnp.broadcast_to(key_gain[:, None], (KD, 128))
     shift = (context_bias + math.log(TOK_DEV / CTX_DEV)) * math.log2(math.e)
     shift = jnp.broadcast_to(shift[:, None], (H, 128))
-    token_rows = call(
+    kv_rows = H * (KD + VDIM)
+    token_rows, ow_all = call(
         attend_kernel,
-        3,
-        jax.ShapeDtypeStruct((T, own_rows, H * VDIM), bf16),
-        VM,
+        2,
+        (
+            jax.ShapeDtypeStruct((T, own_rows, H * VDIM), bf16),
+            jax.ShapeDtypeStruct((Z, CORES) + ow.shape, bf16),
+        ),
+        (VM, ANY),
         [
-            pltpu.VMEM((S,) + kv.shape, bf16), pltpu.VMEM((S,) + ctx.shape, bf16),
+            pltpu.VMEM((Z, CORES) + lat_kv.shape, bf16), pltpu.VMEM((Z, CORES) + query_latent.shape, bf16),
+            pltpu.VMEM((H, block_tokens, 128), bf16), pltpu.VMEM((kv_rows, block_tokens), bf16),
+            pltpu.VMEM((S, kv_rows, block_tokens), bf16), pltpu.VMEM((S,) + ctx.shape, bf16),
             pltpu.VMEM((H, block_tokens, 128), f32), pltpu.VMEM((H, block_tokens, 128), f32),
             pltpu.VMEM((H, block_tokens, VDIM), f32), pltpu.VMEM((block_tokens, H * VDIM), bf16),
-            DMA((S,)), DMA((S,)), DMA((S,)), DMA((S,)), DMA((T,)), DMA((T,)),
+            DMA((2, Z, 2)), DMA((2, Z)), DMA((2, Z + 1)), DMA((2, Z + 1)), DMA((S,)), DMA((S,)),
+            DMA((S,)), DMA((S,)), DMA((S,)), DMA((S,)), DMA((T,)), DMA((T,)), DMA,
         ],
-        (queries, kv, ctx, shift),
+        (lat_kv, query_latent, ow_part, ctx, shift, uq, ukv, pick, gain_q, gain_k, tables),
     )
     token_rows = token_rows.transpose(1, 0, 2).reshape(own_rows, -1)
     projected = jnp.dot(token_rows, ow_all.reshape(-1, width), preferred_element_type=f32)

time: 181 us -> 134 us (0.74)
  other arithmetic: 21 us -> 1.81 us
  local copies, waits for them, and re-layouts: 21.6 us -> 8.39 us
  Pallas kernels: 124 us -> 115 us
  matrix products: 13 us -> 7.5 us
    pallas_call x3 -> x2, Pallas kernels: 124 us -> 115 us  [call(): pl.pallas_call(kernel, out_shape=outs, in_specs=[VM] * len(args), out_spe...]
    concatenate x4 -> x1, local copies, waits for them, and re-layouts: 8.53 us -> 0.01 us  [shards(): act = jnp.concatenate([own_part, jnp.zeros((6, row_span), bf16)], axis=0)]
    dot_general x4 -> x0, matrix products: 4.81 us -> none  [the longest x1 2.5 us: shards(): lax.dot_general(up_key, all_kv, (((0,), (1,)), ((), ())), preferred_eleme...]
    unnamed x39 -> x37, local copies, waits for them, and re-layouts: 1.68 us -> 6.36 us
    another operation x2 -> x1, other arithmetic: 4.44 us -> 0.01 us  [shards(): tables = jnp.stack([table.T for table in tables])]
    reshape x4 -> x0, local copies, waits for them, and re-layouts: 3.76 us -> none  [the longest x1 1.37 us: shards(): uk.reshape(H, NOPE, -1)]
    convert_element_type x3, other arithmetic: 3.25 us -> 0.01 us  [rms_scale(): gain.astype(jnp.float32)]
    mul x1 -> x0, other arithmetic: 2.17 us -> none  [norm_columns(): u * lax.rsqrt(jnp.mean(u * u, axis=-2, keepdims=True) + epsilon)]
where the time goes in v2:
time: 134 us; the launch traced here: 133 us
  Pallas kernels  115 us (86%)
  local copies, waits for them, and re-layouts  8.39 us (6%)
  matrix products  7.5 us (6%)
  other arithmetic  1.81 us (1%)
    pallas_call x2, Pallas kernels, call(): pl.pallas_call(kernel, out_shape=outs, in_specs=[VM] * len(args), out_spe...  115 us
    unnamed x37, local copies, waits for them, and re-layouts  6.36 us
    dot_general x1, matrix products, shards(): jnp.dot(token_rows, ow_all.reshape(-1, width), preferred_element_type=f32)  3.73 us

profile of v2, /device:TPU:0, one launch (start us, length us, event | category | flops | bytes accessed | tf_op | source)
XLA Modules:
  0.0 133.5 jit_solution(8170605095823139234)
XLA Ops:
  0.0 0.7 stack.16
  0.7 0.7 stack.17
  1.5 1.1 copy-done.2
  2.6 1.0 copy-done.3
  3.7 1.0 copy-done.4
  4.7 0.9 copy-done.6
  5.6 39.7 %shard_map.172 = (f32[8,24,256]{2,1,0:T(8,128)S(1)}, bf16[4,2,4,64,768]{4,3,2,1,0:T(8,128)(2,1)}, bf16[4,2,4,64,512]{4,3,2,1,0:T(8,128)(2,1)S(1)}, bf16[4,32,2048]{2,1,0:T(8,128)(2,1)S(1)}) custom-call(bf16[8,512]{1,0:T(8,128)(2,1)S(1)} %concatenate.18.act, bf16[3,512,256]{2,1,0:T(8,128)(2,1)S(1)} %copy-done.2, bf16[4,64,768]{2,1,0:T(8,128)(2,1)S(1)} %bitcast.29, ...), custom_call_target="tpu_custom_call" | custom-call | tf_op jit(solution)/shard_map/pallas_call | solution.py:512
  45.4 0.2 fusion.2
  45.6 0.3 fusion.6
  45.9 0.1 fusion.9
  46.0 0.1 fusion.13
  46.2 0.6 multiply_reduce_fusion.1
  46.9 0.1 fusion.17
  47.2 0.3 convolution_convert_fusion
  47.5 0.2 multiply_reduce_fusion.2
  47.8 0.1 multiply_convert_fusion.2
  47.9 0.1 convolution_convert_fusion.1
  48.3 2.6 %multiply_reduce_fusion = (f32[128]{0:T(128)S(1)}, f32[128,768]{1,0:T(8,128)S(1)}) fusion(bf16[128,2048]{1,0:T(8,128)(2,1)S(1)} %fusion.6, bf16[2048,768]{1,0:T(8,128)(2,1)} %bitcast.36), kind=kOutput, calls=%fused_computation.15 | convolution fusion | flops 402849664 | bytes 4063744 | tf_op jit(solution)/shard_map/dot_general | solution.py:563
  51.0 0.3 multiply_cosine_fusion.1
  51.4 0.1 copy.23
  51.9 75.7 %shard_map.173 = (bf16[8,128,128]{2,1,0:T(8,128)(2,1)S(1)}, bf16[4,2,4,32,2048]{4,3,2,1,0:T(8,128)(2,1)S(1)}) custom-call(bf16[128,640]{1,0:T(8,128)(2,1)S(1)} %fusion.14.lat_kv, bf16[128,768]{1,0:T(8,128)(2,1)S(1)} %multiply_convert_fusion.lat_q, bf16[4,32,2048]{2,1,0:T(8,128)(2,1)S(1)} %get-tuple-element.14.ow_part, bf16[32,512]{1,0:T(8,128)(2,1)S(1)} %bitcast.33, ...), custom_call_target="tpu_custom_call" | custom-call | tf_op jit(solution)/shard_map/pallas_call | solution.py:512
  127.6 1.9 %copy-done.1 = bf16[4,2,4,32,2048]{4,3,2,1,0:T(8,128)(2,1)} copy-done((bf16[4,2,4,32,2048]{4,3,2,1,0:T(8,128)(2,1)}, bf16[4,2,4,32,2048]{4,3,2,1,0:T(8,128)(2,1)S(1)}, u32[]{:S(2)}) %copy-start.1) | copy-done | bytes 4194328
  129.6 0.2 copy.25
  129.7 3.7 %fusion.1 = bf16[128,2048]{1,0:T(8,128)(2,1)} fusion(bf16[128,1024]{0,1:T(8,128)(2,1)S(1)} %bitcast.37, bf16[1024,2048]{1,0:T(8,128)(2,1)} %bitcast.27, bf16[128,2048]{1,0:T(8,128)(2,1)S(1)} %copy-done.7, f32[2048]{0:T(1024)S(1)} %bitcast.39), kind=kOutput, calls=%fused_computation.2 | convolution fusion | flops 537919488 | bytes 5513216 | tf_op jit(solution)/shard_map/dot_general | solution.py:612
  (62 shorter events, 1.1 us)
Async XLA Ops:
  0.0 47.2 %copy-start = (bf16[2048,32]{0,1:T(8,128)(2,1)S(1)}, bf16[2048,32]{0,1:T(8,128)(2,1)}, u32[]{:S(2)}) copy-start(bf16[2048,32]{0,1:T(8,128)(2,1)} %param.26) | copy-start | bytes 393220
  0.0 45.3 %copy-start.11 = (bf16[2048]{0:T(1024)(128)(2,1)S(1)}, bf16[2048]{0:T(1024)(128)(2,1)}, u32[]{:S(2)}) copy-start(bf16[2048]{0:T(1024)(128)(2,1)} %param.23) | copy-start | bytes 12292
  1.5 1.1 copy-start.2
  2.6 1.0 copy-start.3
  3.7 1.0 copy-start.4
  4.7 0.9 copy-start.6
  5.6 39.7 %copy-start.7 = (bf16[128,2048]{1,0:T(8,128)(2,1)S(1)}, bf16[128,2048]{1,0:T(8,128)(2,1)}, u32[]{:S(2)}) copy-start(bf16[128,2048]{1,0:T(8,128)(2,1)} %param.18) | copy-start | bytes 1572868
  5.6 40.2 %copy-start.8 = (bf16[32,2048]{1,0:T(8,128)(2,1)S(1)}, bf16[32,2048]{1,0:T(8,128)(2,1)}, u32[]{:S(2)}) copy-start(bf16[32,2048]{1,0:T(8,128)(2,1)} %param.19) | copy-start | bytes 393220
  45.9 1.0 copy-start.14
  46.0 0.9 copy-start.9
  46.2 1.6 %copy-start.12 = (f32[96]{0:T(128)S(1)}, f32[96]{0:T(128)}, u32[]{:S(2)}) copy-start(f32[96]{0:T(128)} %param.33) | copy-start | bytes 1156
  46.2 1.7 %copy-start.10 = (bf16[512,128]{1,0:T(8,128)(2,1)S(1)}, bf16[512,128]{1,0:T(8,128)(2,1)}, u32[]{:S(2)}) copy-start(bf16[512,128]{1,0:T(8,128)(2,1)} %param.31) | copy-start | bytes 393220
  48.3 2.6 %copy-start.13 = (bf16[768]{0:T(1024)(128)(2,1)S(1)}, bf16[768]{0:T(1024)(128)(2,1)}, u32[]{:S(2)}) copy-start(bf16[768]{0:T(1024)(128)(2,1)} %param.27) | copy-start | bytes 4612
  48.3 3.4 %copy-start.15 = (f32[96]{0:T(128)S(1)}, f32[96]{0:T(128)}, u32[]{:S(2)}) copy-start(f32[96]{0:T(128)} %param.32) | copy-start | bytes 1156
  50.8 1.0 copy-start.16
  50.9 1.1 copy-start.5
  127.6 1.9 %copy-start.1 = (bf16[4,2,4,32,2048]{4,3,2,1,0:T(8,128)(2,1)}, bf16[4,2,4,32,2048]{4,3,2,1,0:T(8,128)(2,1)S(1)}, u32[]{:S(2)}) copy-start(bf16[4,2,4,32,2048]{4,3,2,1,0:T(8,128)(2,1)S(1)} %get-tuple-element.16) | copy-start | bytes 12582916

commit v3 on v2

--- a/solution.py
+++ b/solution.py
@@ -346,8 +346,9 @@
         to = ow_all.at[:, core, lax.rem(sp - k + S, S)]
         return remote(ow_part, to, s_send.at[k], s_recv.at[k], {"sp": lax.rem(sp + k, S)})
 
+    early = 1 + 2 * (S - 1) // 3
     loop(1, S, lambda k: ctx_copy(k).start())
-    loop(1, S, lambda k: spread(k).start())
+    loop(1, early, lambda k: spread(k).start())
     own_ow = pltpu.make_async_copy(ow_part, ow_all.at[:, core, sp], loc)
     own_ow.start()
     ctx_all[sp] = ctx[...]
@@ -389,6 +390,7 @@
 
     loop(0, Z, expand_kv)
     loop(1, S, lambda k: kv_copy(k).start())
+    loop(early, S, lambda k: spread(k).start())
     passed(1)
 
     def expand_q(b):
@@ -463,31 +465,31 @@
 
         loop(0, N // TQ, tile)
 
+    loop(1, S, latent_step)
+
+    def finish(qi):
+        at = pl.ds(pl.multiple_of(qi * TQ, TQ), TQ)
+        heads = [acc[h, at, :] / jnp.sum(l_scr[h, at, :], axis=1, keepdims=True) for h in range(H)]
+        att[at, :] = jnp.concatenate(heads, axis=1).astype(jnp.bfloat16)
+
+    loop(0, N // TQ, finish)
+
+    def give(k):
+        peer = lax.rem(tp + k, T)
+        return remote(
+            att.at[pl.ds(pl.multiple_of(peer * rows, rows), rows)], out.at[tp], a_send.at[k], a_recv.at[k], {"tp": peer}
+        )
+
+    def take(k):
+        to = out.at[lax.rem(tp - k + T, T)]
+        remote(to, to, a_send.at[k], a_recv.at[k], {"tp": lax.rem(tp + k, T)}).wait_recv()
+
+    loop(1, T, lambda k: give(k).start())
     own_ow.wait()
     loop(1, S, lambda k: gathered(k).wait_recv())
     half = ow_all.at[:, core]
     whole = remote(half, half, c_send.at[0, Z], c_recv.at[0, Z], mate)
     whole.start()
-    loop(1, S, latent_step)
-
-    def finish(qi):
-        at = pl.ds(pl.multiple_of(qi * TQ, TQ), TQ)
-        heads = [acc[h, at, :] / jnp.sum(l_scr[h, at, :], axis=1, keepdims=True) for h in range(H)]
-        att[at, :] = jnp.concatenate(heads, axis=1).astype(jnp.bfloat16)
-
-    loop(0, N // TQ, finish)
-
-    def give(k):
-        peer = lax.rem(tp + k, T)
-        return remote(
-            att.at[pl.ds(pl.multiple_of(peer * rows, rows), rows)], out.at[tp], a_send.at[k], a_recv.at[k], {"tp": peer}
-        )
-
-    def take(k):
-        to = out.at[lax.rem(tp - k + T, T)]
-        remote(to, to, a_send.at[k], a_recv.at[k], {"tp": lax.rem(tp + k, T)}).wait_recv()
-
-    loop(1, T, lambda k: give(k).start())
     out[tp] = att[pl.ds(pl.multiple_of(tp * rows, rows), rows), :]
     loop(1, T, take)
     loop(1, T, lambda k: give(k).wait_send())
@@ -508,11 +510,11 @@
 ANY = pl.BlockSpec(memory_space=pl.ANY)
 
 
-def call(kernel, ident, outs, out_specs, scratch, args):
+def call(kernel, ident, outs, out_specs, scratch, args, in_specs=None):
     return pl.pallas_call(
         kernel,
         out_shape=outs,
-        in_specs=[VM] * len(args),
+        in_specs=in_specs or [VM] * len(args),
         out_specs=out_specs,
         scratch_shapes=scratch,
         compiler_params=pltpu.CompilerParams(
@@ -554,6 +556,7 @@
             DMA((3, Z, 2)), DMA((3, Z)), DMA((2, Z, S)), DMA((2, Z, S)), DMA((2, Z)), DMA((2, Z)), DMA((3,)),
         ],
         (act, mod_weight, dq, dkv, ow),
+        [VM, VM, ANY, ANY, ANY],
     )
     mods = mods.transpose(1, 0, 2).reshape(24, width)
     normed = modulate(latent, norm_gain, mods[0], mods[8])

time: 134 us -> 139 us (1.037)
  the two profiles are of different devices: /device:TPU:0 before, /device:TPU:3 now
where the time goes in v3:
time: 139 us; the launch traced here: 138 us
  Pallas kernels  120 us (86%)
  local copies, waits for them, and re-layouts  8.39 us (6%)
  matrix products  7.49 us (5%)
  other arithmetic  1.81 us (1%)
    pallas_call x2, Pallas kernels, call(): pl.pallas_call(kernel, out_shape=outs, in_specs=in_specs or [VM] * len(ar...  120 us
    unnamed x37, local copies, waits for them, and re-layouts  6.36 us
    dot_general x1, matrix products, shards(): jnp.dot(token_rows, ow_all.reshape(-1, width), preferred_element_type=f32)  3.73 us

profile of v3, /device:TPU:3, one launch (start us, length us, event | category | flops | bytes accessed | tf_op | source)
XLA Modules:
  0.0 138.4 jit_solution(7650232374972198258)
XLA Ops:
  0.0 0.7 stack.16
  0.7 0.7 stack.17
  1.5 1.1 copy-done.2
  2.6 1.0 copy-done.3
  3.7 1.0 copy-done.4
  4.7 0.9 copy-done.6
  5.6 39.8 %shard_map.172 = (f32[8,24,256]{2,1,0:T(8,128)S(1)}, bf16[4,2,4,64,768]{4,3,2,1,0:T(8,128)(2,1)}, bf16[4,2,4,64,512]{4,3,2,1,0:T(8,128)(2,1)S(1)}, bf16[4,32,2048]{2,1,0:T(8,128)(2,1)S(1)}) custom-call(bf16[8,512]{1,0:T(8,128)(2,1)S(1)} %concatenate.18.act, bf16[3,512,256]{2,1,0:T(8,128)(2,1)S(1)} %copy-done.2, bf16[4,64,768]{2,1,0:T(8,128)(2,1)S(1)} %bitcast.29, ...), custom_call_target="tpu_custom_call" | custom-call | tf_op jit(solution)/shard_map/pallas_call | solution.py:514
  45.5 0.2 fusion.2
  45.7 0.3 fusion.6
  46.0 0.1 fusion.9
  46.2 0.1 fusion.13
  46.3 0.6 multiply_reduce_fusion.1
  47.1 0.1 fusion.17
  47.3 0.3 convolution_convert_fusion
  47.7 0.2 multiply_reduce_fusion.2
  47.9 0.1 multiply_convert_fusion.2
  48.0 0.1 convolution_convert_fusion.1
  48.4 2.6 %multiply_reduce_fusion = (f32[128]{0:T(128)S(1)}, f32[128,768]{1,0:T(8,128)S(1)}) fusion(bf16[128,2048]{1,0:T(8,128)(2,1)S(1)} %fusion.6, bf16[2048,768]{1,0:T(8,128)(2,1)} %bitcast.36), kind=kOutput, calls=%fused_computation.15 | convolution fusion | flops 402849664 | bytes 4063744 | tf_op jit(solution)/shard_map/dot_general | solution.py:566
  51.2 0.3 multiply_cosine_fusion.1
  51.5 0.1 copy.23
  52.1 80.4 %shard_map.173 = (bf16[8,128,128]{2,1,0:T(8,128)(2,1)S(1)}, bf16[4,2,4,32,2048]{4,3,2,1,0:T(8,128)(2,1)S(1)}) custom-call(bf16[128,640]{1,0:T(8,128)(2,1)S(1)} %fusion.14.lat_kv, bf16[128,768]{1,0:T(8,128)(2,1)S(1)} %multiply_convert_fusion.lat_q, bf16[4,32,2048]{2,1,0:T(8,128)(2,1)S(1)} %get-tuple-element.14.ow_part, bf16[32,512]{1,0:T(8,128)(2,1)S(1)} %bitcast.33, ...), custom_call_target="tpu_custom_call" | custom-call | tf_op jit(solution)/shard_map/pallas_call | solution.py:514
  132.5 1.9 %copy-done.1 = bf16[4,2,4,32,2048]{4,3,2,1,0:T(8,128)(2,1)} copy-done((bf16[4,2,4,32,2048]{4,3,2,1,0:T(8,128)(2,1)}, bf16[4,2,4,32,2048]{4,3,2,1,0:T(8,128)(2,1)S(1)}, u32[]{:S(2)}) %copy-start.1) | copy-done | bytes 4194328
  134.4 0.2 copy.25
  134.6 3.7 %fusion.1 = bf16[128,2048]{1,0:T(8,128)(2,1)} fusion(bf16[128,1024]{0,1:T(8,128)(2,1)S(1)} %bitcast.37, bf16[1024,2048]{1,0:T(8,128)(2,1)} %bitcast.27, bf16[128,2048]{1,0:T(8,128)(2,1)S(1)} %copy-done.7, f32[2048]{0:T(1024)S(1)} %bitcast.39), kind=kOutput, calls=%fused_computation.2 | convolution fusion | flops 537919488 | bytes 5513216 | tf_op jit(solution)/shard_map/dot_general | solution.py:615
  (62 shorter events, 1.1 us)
Async XLA Ops:
  0.0 47.3 %copy-start = (bf16[2048,32]{0,1:T(8,128)(2,1)S(1)}, bf16[2048,32]{0,1:T(8,128)(2,1)}, u32[]{:S(2)}) copy-start(bf16[2048,32]{0,1:T(8,128)(2,1)} %param.26) | copy-start | bytes 393220
  0.0 45.5 %copy-start.11 = (bf16[2048]{0:T(1024)(128)(2,1)S(1)}, bf16[2048]{0:T(1024)(128)(2,1)}, u32[]{:S(2)}) copy-start(bf16[2048]{0:T(1024)(128)(2,1)} %param.23) | copy-start | bytes 12292
  1.5 1.1 copy-start.2
  2.6 1.0 copy-start.3
  3.7 1.0 copy-start.4
  4.7 0.9 copy-start.6
  5.6 39.9 %copy-start.7 = (bf16[128,2048]{1,0:T(8,128)(2,1)S(1)}, bf16[128,2048]{1,0:T(8,128)(2,1)}, u32[]{:S(2)}) copy-start(bf16[128,2048]{1,0:T(8,128)(2,1)} %param.18) | copy-start | bytes 1572868
  5.6 40.4 %copy-start.8 = (bf16[32,2048]{1,0:T(8,128)(2,1)S(1)}, bf16[32,2048]{1,0:T(8,128)(2,1)}, u32[]{:S(2)}) copy-start(bf16[32,2048]{1,0:T(8,128)(2,1)} %param.19) | copy-start | bytes 393220
  46.0 1.0 copy-start.14
  46.2 0.9 copy-start.9
  46.3 1.6 %copy-start.12 = (f32[96]{0:T(128)S(1)}, f32[96]{0:T(128)}, u32[]{:S(2)}) copy-start(f32[96]{0:T(128)} %param.33) | copy-start | bytes 1156
  46.3 1.7 %copy-start.10 = (bf16[512,128]{1,0:T(8,128)(2,1)S(1)}, bf16[512,128]{1,0:T(8,128)(2,1)}, u32[]{:S(2)}) copy-start(bf16[512,128]{1,0:T(8,128)(2,1)} %param.31) | copy-start | bytes 393220
  48.4 2.6 %copy-start.13 = (bf16[768]{0:T(1024)(128)(2,1)S(1)}, bf16[768]{0:T(1024)(128)(2,1)}, u32[]{:S(2)}) copy-start(bf16[768]{0:T(1024)(128)(2,1)} %param.27) | copy-start | bytes 4612
  48.4 3.4 %copy-start.15 = (f32[96]{0:T(128)S(1)}, f32[96]{0:T(128)}, u32[]{:S(2)}) copy-start(f32[96]{0:T(128)} %param.32) | copy-start | bytes 1156
  51.0 1.0 copy-start.16
  51.0 1.1 copy-start.5
  132.5 1.9 %copy-start.1 = (bf16[4,2,4,32,2048]{4,3,2,1,0:T(8,128)(2,1)}, bf16[4,2,4,32,2048]{4,3,2,1,0:T(8,128)(2,1)S(1)}, u32[]{:S(2)}) copy-start(bf16[4,2,4,32,2048]{4,3,2,1,0:T(8,128)(2,1)S(1)} %get-tuple-element.16) | copy-start | bytes 12582916
